TPU v7x, 32 devices: a whole 2x2x4 slice. The times are simulated.
32 devices in a mesh: grp: 2 (over y), ep: 4 (over z), tp: 4 (over x, core).
Axes of the slice: x: 2, y: 2, z: 4, core: 2. Of those that a mesh axis runs over, the one named last changes fastest.
Arguments:
- queries: bfloat16 [1024, 2048], P(('grp', 'ep'), 'tp'), parts along dimension 0, may hold values from -6 to 6
- keys: bfloat16 [1024, 2048], P(('grp', 'ep'), 'tp'), parts along dimension 0, may hold values from -6 to 6
- values: bfloat16 [1024, 2048], P(('grp', 'ep'), 'tp'), parts along dimension 0, may hold values from -6 to 6
- stop_bias: bfloat16 [1024, 32], P(('grp', 'ep'), 'tp'), parts along dimension 0, may hold values from -20 to 0
- out_weight: bfloat16 [2048, 2048], P('tp'), may hold values from -0.125 to 0.125
- mix_gain: float32 [2048], replicated, may hold values from 0.1 to 1.9
- moe_input: bfloat16 [4096, 2048], P(('grp', 'ep', 'tp')), parts along dimension 0, may hold values from -6 to 6
- ffn_gain: float32 [2048], replicated, may hold values from 0.1 to 1.9
- expert_ids: int32 [4096, 2], P(('grp', 'ep', 'tp')), parts along dimension 0, may hold values from 0 to 3, all different within a row; in each aligned block of 128 rows (0 to 127, 128 to 255, ...) at most 96 rows name the same one
- expert_scores: float32 [4096, 2], P(('grp', 'ep', 'tp')), parts along dimension 0, may hold values from 0.05 to 1
- gate_weight: bfloat16 [4, 2048, 1024], P('ep', None, 'tp'), may hold values from -0.125 to 0.125
- up_weight: bfloat16 [4, 2048, 1024], P('ep', None, 'tp'), may hold values from -0.125 to 0.125
- down_weight: bfloat16 [4, 1024, 2048], P('ep', 'tp'), may hold values from -0.1875 to 0.1875
Outputs:
- mixed: bfloat16 [1024, 2048], P(('grp', 'ep', 'tp')), parts along dimension 0
- experts_mixed: bfloat16 [4096, 2048], P(('grp', 'ep', 'tp')), parts along dimension 0
There are 2 independent parts, one for each index of `grp`. A program takes and returns all parts, laid end to end along the dimension named above; an argument that names none is the same for every part. Nothing has to cross between parts.
Inputs may be any that keep to these rules, and one draw needn't show every extreme that they name: `expert_ids`: each token names 2 different experts. Among the 128 tokens of one device, no expert is named by more than 96 tokens, and in some device's tokens some expert is named by exactly 96.
All inputs are finite; a program needn't handle non-finite values.
Results may differ from a plain program's by a relative error of at most 0.012.
Values may be sent and summed in bfloat16 or wider, within the bound.
A program may use at most 128 MiB of HBM per device.

v0:
```python
import functools

import jax
import jax.numpy as jnp
from jax import lax
from jax.experimental import pallas as pl
from jax.experimental.pallas import tpu as pltpu
from jax.sharding import PartitionSpec as P

MESH = pl.DeviceIdType.MESH
F32 = jnp.float32
BF16 = jnp.bfloat16


def norm_rows(values, gain):
    values = values.astype(jnp.float32)
    scale = lax.rsqrt(jnp.mean(values * values, axis=-1, keepdims=True) + 1e-06)
    return values * scale * gain


def break_terms(query_heads, query_place, key_block, bias_block, first):
    span = key_block.shape[0]
    heads = query_heads.shape[1]
    key_heads = key_block.reshape(span, heads, -1)
    scores = jnp.einsum("qhd,khd->hqk", query_heads, key_heads, preferred_element_type=jnp.float32)
    scores = scores * query_heads.shape[2] ** (-0.5) + bias_block.astype(jnp.float32).T[:, None, :]
    key_place = first + jnp.arange(span)
    past = (key_place[None, :] < query_place[:, None])[None]
    rest = jnp.where(past, jax.nn.log_sigmoid(-scores), 0.0)
    later = lax.cumsum(rest, axis=2, reverse=True)
    return (scores, past, rest, later)


def block_part(scores, past, rest, later, value_block, heads):
    within = later - rest
    local = jnp.where(past, jnp.exp(jax.nn.log_sigmoid(scores) + within), 0.0).astype(jnp.bfloat16)
    span = value_block.shape[0]
    value_heads = value_block.reshape(span, heads, -1)
    part = jnp.einsum("hqk,khd->qhd", local, value_heads, preferred_element_type=jnp.float32)
    return part.reshape(part.shape[0], -1)


def keep(state):
    return state


def dispatch_plan(normed, expert_ids, experts, capacity):
    rows, top = expert_ids.shape
    flat_ids = expert_ids.reshape(rows * top)
    onehot = (flat_ids[:, None] == jnp.arange(experts)[None, :]).astype(jnp.int32)
    earlier = jnp.cumsum(onehot, axis=0) - onehot
    place = jnp.sum(earlier * onehot, axis=1)
    target = flat_ids * capacity + place
    source = (
        jnp.zeros((experts * capacity,), jnp.int32)
        .at[target]
        .set(jnp.arange(rows * top, dtype=jnp.int32) // top + 1)
    )
    padded = jnp.concatenate([jnp.zeros((1, normed.shape[1]), normed.dtype), normed], axis=0)
    return (padded[source].reshape(experts, capacity, normed.shape[1]), target)


def expert_hidden(piece, gate_weight, up_weight):
    flat = piece.reshape(-1, piece.shape[-1])
    gate = jnp.dot(flat, gate_weight[0], preferred_element_type=jnp.float32)
    upward = jnp.dot(flat, up_weight[0], preferred_element_type=jnp.float32)
    hidden = (jax.nn.silu(gate) * upward).astype(jnp.bfloat16)
    return hidden.reshape(piece.shape[0], piece.shape[1], -1)


def send_back(summed):
    return lax.all_to_all(
        summed.astype(jnp.bfloat16), "ep", split_axis=0, concat_axis=0, tiled=True
    )


def return_rows(hidden_all, down_weight, sources):
    flat = hidden_all.reshape(-1, hidden_all.shape[2])
    product = jnp.dot(flat, down_weight[0], preferred_element_type=jnp.float32)
    return send_back(
        lax.psum_scatter(
            product.reshape(sources * lax.axis_size("tp"), hidden_all.shape[1], -1).astype(
                jnp.bfloat16
            ),
            "tp",
            scatter_dimension=0,
            tiled=True,
        ).astype(jnp.float32)
    )


def per_device(
    queries,
    keys,
    values,
    stop_bias,
    out_weight,
    mix_gain,
    moe_input,
    ffn_gain,
    expert_ids,
    expert_scores,
    gate_weight,
    up_weight,
    down_weight,
):
    span = queries.shape[0]
    heads = stop_bias.shape[1]
    width_heads = queries.shape[1]
    blocks = lax.axis_size("ep")
    own_first = lax.axis_index("ep") * span
    query_heads = queries.reshape(span, heads, -1)
    query_place = own_first + jnp.arange(span)

    def piece_rows(piece, index):
        return tuple((lax.dynamic_slice_in_dim(member, index * span, span, 0) for member in piece))

    start_state = (
        jnp.zeros((blocks, heads, span), jnp.float32),
        jnp.zeros((blocks, span, width_heads), jnp.float32),
    )
    piece = (
        lax.all_gather(keys, "ep", axis=0, tiled=True),
        lax.all_gather(values, "ep", axis=0, tiled=True),
        lax.all_gather(stop_bias, "ep", axis=0, tiled=True),
    )

    def one_block(index, state):
        key_block, value_block, bias_block = piece_rows(piece, index)
        first = index * span

        def compute(inner_state):
            totals, parts = inner_state
            scores, past, rest, later = break_terms(
                query_heads, query_place, key_block, bias_block, first
            )
            part = block_part(scores, past, rest, later, value_block, heads)
            number = first // span
            totals = lax.dynamic_update_index_in_dim(totals, later[:, :, 0], number, 0)
            parts = lax.dynamic_update_index_in_dim(parts, part, number, 0)
            return (totals, parts)

        return lax.cond(first <= own_first, compute, keep, state)

    totals, parts = lax.fori_loop(0, piece[0].shape[0] // span, one_block, start_state)
    carried = lax.cumsum(totals, axis=0, reverse=True) - totals
    factor = jnp.exp(carried).transpose(0, 2, 1)[:, :, :, None]
    attended = jnp.sum(factor * parts.reshape(blocks, span, heads, -1), axis=0).reshape(
        span, width_heads
    )
    attended = attended.astype(jnp.bfloat16)
    projected = lax.psum_scatter(
        jnp.dot(attended, out_weight, preferred_element_type=jnp.float32).astype(jnp.bfloat16),
        "tp",
        scatter_dimension=0,
        tiled=True,
    ).astype(jnp.float32)
    mixed = norm_rows(projected, mix_gain).astype(jnp.bfloat16)
    normed = norm_rows(moe_input, ffn_gain).astype(jnp.bfloat16)
    rows, top = expert_ids.shape
    experts = lax.axis_size("ep")
    capacity = 3 * rows * top // (2 * experts)
    weights = expert_scores / jnp.sum(expert_scores, axis=1, keepdims=True)
    outbound, target = dispatch_plan(normed, expert_ids, experts, capacity)
    arrived = lax.all_to_all(outbound, "ep", split_axis=0, concat_axis=0, tiled=True)
    hidden_all = expert_hidden(
        lax.all_gather(arrived, "tp", axis=0, tiled=True), gate_weight, up_weight
    )
    returned = return_rows(hidden_all, down_weight, arrived.shape[0])
    picked = returned.reshape(experts * capacity, -1)[target].reshape(rows, top, -1)
    experts_mixed = jnp.sum(picked.astype(jnp.float32) * weights[:, :, None], axis=1).astype(
        jnp.bfloat16
    )
    return (mixed, experts_mixed)


def contract_rows(left, right):
    return lax.dot_general(left, right, (((0,), (0,)), ((), ())), preferred_element_type=F32)


def layer_kernel(
    ep,
    capacity,
    head,
    q_ref,
    k_ref,
    v_ref,
    bias_ref,
    ow_ref,
    mix_gain_ref,
    x_ref,
    ffn_gain_ref,
    ids_ref,
    scores_ref,
    g_ref,
    u_ref,
    d_ref,
    mixed_ref,
    out_ref,
    q_all,
    k_all,
    v_all,
    bias_all,
    bias_rows,
    att_send,
    att_all,
    proj,
    proj_in,
    ow,
    meta,
    meta_in,
    normed_ref,
    dense_in,
    sel,
    gate_cols,
    outbound,
    relay_out,
    rows_in,
    acc,
    back_out,
    back_in,
    outer_out,
    outer_in,
    dense_out,
    dense_back,
    g_far,
    u_far,
    d_far,
    ow_sem,
    pack_send,
    pack_recv,
    row_send,
    row_recv,
    meta_send,
    meta_recv,
    dense_send,
    dense_recv,
    relay_send,
    relay_recv,
    att_ssem,
    att_rsem,
    back_ssem,
    back_rsem,
    outer_send,
    outer_recv,
    home_send,
    home_recv,
    proj_ssem,
    proj_rsem,
    near_send,
    near_recv,
    x_send,
    x_recv,
    y_send,
    y_recv,
    fwd_send,
    fwd_recv,
):
    me = lax.axis_index("ep")
    tp = lax.axis_index("tp")
    grp = lax.axis_index("grp")
    chip, core = tp // 2, tp % 2
    mates = [None, chip * 2 + (1 - core), (1 - chip) * 2 + core, (1 - chip) * 2 + (1 - core)]
    span = q_ref.shape[0]
    width = q_all.shape[2]
    heads = width // head

    half = me // 2
    inner = lax.rem(me + 1, ep) >= 2
    side = me + 1 - 2 * (me % 2)
    far_inner = 2 - half
    far_base = 2 * (1 - half)
    ow_copy = pltpu.make_async_copy(ow_ref, ow, ow_sem)
    ow_copy.start()

    barrier = pltpu.get_barrier_semaphore()
    peers = [{"ep": lax.rem(me + r, ep)} for r in range(1, ep)]
    peers += [{"tp": mates[m]} for m in (1, 2, 3)] + [{"grp": 1 - grp}]
    for peer in peers:
        pl.semaphore_signal(barrier, inc=1, device_id=peer, device_id_type=MESH)
    pl.semaphore_wait(barrier, len(peers))

    def send(src, dst, ssem, rsem, peer):
        return pltpu.make_async_remote_copy(
            src_ref=src,
            dst_ref=dst,
            send_sem=ssem,
            recv_sem=rsem,
            device_id=peer,
            device_id_type=MESH,
        )

    weights = (g_ref, u_ref, d_ref)
    fars = (g_far, u_far, d_far)
    started = []

    def go(copy):
        copy.start()
        started.append(copy)
        return copy

    cuts = g_ref.shape[1]
    chunks = [(c, a) for c in range(cuts) for a in range(2)] + [(c, 2) for c in range(cuts)]
    over_x = {}
    for n, (c, a) in enumerate(chunks):
        over_x[n] = go(
            send(
                weights[a].at[grp, c],
                fars[a].at[1, grp, c],
                x_send.at[n],
                x_recv.at[n],
                {"tp": mates[2]},
            )
        )
    near = [
        go(
            send(
                weights[a], fars[a].at[0], near_send.at[a], near_recv.at[a], {"tp": mates[1]}
            )
        )
        for a in range(3)
    ]
    tokens, deep = x_ref.shape
    top = ids_ref.shape[0]
    scores = scores_ref[...]
    gates = scores / jnp.sum(scores, axis=0, keepdims=True)
    meta[...] = jnp.zeros_like(meta)
    meta[0:top] = ids_ref[...].astype(F32)
    meta[top : 2 * top] = gates
    go(send(meta, meta_in.at[me % 2], meta_send, meta_recv.at[me % 2], {"ep": far_inner}))
    values = x_ref[...].astype(F32)
    scale = lax.rsqrt(jnp.mean(values * values, axis=-1, keepdims=True) + 1e-06)
    normed = (values * scale * ffn_gain_ref[...]).astype(BF16)
    normed_ref[...] = normed
    parts = dense_send.shape[0]
    step_cols = deep // parts

    def cols_of(c):
        return slice(c * step_cols, (c + 1) * step_cols)

    for c in range(parts):
        go(
            send(
                normed_ref.at[:, cols_of(c)],
                dense_in.at[me % 2, :, cols_of(c)],
                dense_send.at[c],
                dense_recv.at[me % 2, c],
                {"ep": far_inner},
            )
        )
    square = (tokens, tokens)
    lane = lax.broadcasted_iota(jnp.int32, square, 1)
    sub = lax.broadcasted_iota(jnp.int32, square, 0)
    earlier = (sub < lane).astype(BF16)
    slot = lax.broadcasted_iota(jnp.int32, (capacity, tokens), 0).astype(F32)

    def route(table, first, second, at):
        named = jnp.zeros(square, F32)
        gate = jnp.zeros(square, F32)
        for n, e in enumerate((first, second)):
            place_of = e.astype(F32)
            for k in range(top):
                hit = table[k : k + 1, :] == place_of
                here = sub == n
                named = named + jnp.where(here & hit, 1.0, 0.0)
                gate = gate + jnp.where(here & hit, table[top + k : top + k + 1, :], 0.0)
        place = jnp.dot(named.astype(BF16), earlier, preferred_element_type=F32)
        for n in range(2):
            sel[2 * at + n] = jnp.where(
                slot == place[n : n + 1, :], named[n : n + 1, :], 0.0
            ).astype(BF16)
        gate_cols[at] = gate.T

    def pick(n, block):
        return jnp.dot(sel[n], block, preferred_element_type=F32).astype(BF16)

    route(meta[...], me, side, 0)
    outbound[...] = pick(1, normed)
    side_rows = go(send(outbound, rows_in.at[1], row_send, row_recv, {"ep": side}))
    rows_in[0] = pick(0, normed)

    def dense_of(q, c):
        return send(
            normed_ref.at[:, cols_of(c)],
            dense_in.at[q, :, cols_of(c)],
            dense_send.at[c],
            dense_recv.at[q, c],
            {"ep": far_inner},
        )

    def relay_of(q, c):
        return send(
            relay_out.at[q, :, cols_of(c)],
            rows_in.at[2 + q, :, cols_of(c)],
            relay_send.at[q, c],
            relay_recv.at[q, c],
            {"ep": side},
        )

    def relay(c):
        @pl.when(inner)
        def _():
            for q in range(2):
                if c == 0:
                    send(
                        meta, meta_in.at[q], meta_send, meta_recv.at[q], {"ep": far_inner}
                    ).wait_recv()
                    route(meta_in[q], me, side, 1 + q)
                dense_of(q, c).wait_recv()
                block = dense_in[q, :, cols_of(c)]
                relay_out[q, :, cols_of(c)] = pick(2 * (1 + q) + 1, block)
                relay_of(q, c).start()
                rows_in[2 + q, :, cols_of(c)] = pick(2 * (1 + q), block)

    packs = {}
    for r in (2, 1, 3)[: ep - 1]:
        dest = lax.rem(me + r, ep)
        cols = pl.ds(pl.multiple_of(dest * width, width), width)
        pieces = (
            (q_ref.at[:, cols], q_all.at[me]),
            (k_ref.at[:, cols], k_all.at[me]),
            (v_ref.at[:, cols], v_all.at[me]),
            (bias_ref, bias_all.at[me]),
        )
        packs[r] = [
            go(send(s, t, pack_send.at[r, n], pack_recv.at[r, n], {"ep": dest}))
            for n, (s, t) in enumerate(pieces)
        ]
    own = pl.ds(pl.multiple_of(me * width, width), width)
    q_all[me] = q_ref[:, own]
    k_all[me] = k_ref[:, own]
    v_all[me] = v_ref[:, own]
    bias_all[me] = bias_ref[...]

    over_y, cross = {}, {}

    def forward(n):
        c, a = chunks[n]
        over_x[n].wait_recv()
        over_y[n] = go(
            send(
                fars[a].at[1, grp, c],
                fars[a].at[1, grp, c],
                y_send.at[n],
                y_recv.at[n],
                {"grp": 1 - grp},
            )
        )
        cross[0, n] = go(
            send(
                fars[a].at[1, grp, c],
                fars[a].at[2, grp, c],
                fwd_send.at[0, n],
                fwd_recv.at[0, n],
                {"tp": mates[1]},
            )
        )

    def forward_again(n):
        c, a = chunks[n]
        over_y[n].wait_recv()
        cross[1, n] = go(
            send(
                fars[a].at[1, 1 - grp, c],
                fars[a].at[2, 1 - grp, c],
                fwd_send.at[1, n],
                fwd_recv.at[1, n],
                {"tp": mates[1]},
            )
        )

    block = (span, span)
    key_sub = lax.broadcasted_iota(jnp.int32, block, 0)
    key_lane = lax.broadcasted_iota(jnp.int32, block, 1)
    after = (key_sub > key_lane).astype(BF16)

    def attend(i):
        def one(step, state):
            j = i - step
            past = (j * span + key_lane) < (i * span + key_sub)
            result = []
            for h in range(heads):
                total, carry = state[2 * h], state[2 * h + 1]
                cols = slice(h * head, (h + 1) * head)
                z = lax.dot_general(
                    q_all[i][:, cols],
                    k_all[j][:, cols],
                    (((1,), (1,)), ((), ())),
                    preferred_element_type=F32,
                )
                z = z * head ** (-0.5) + bias_rows[j, pl.ds(me * heads + h, 1), :]
                soft = jnp.log1p(jnp.exp(-jnp.abs(z)))
                stay = -(jnp.maximum(z, 0.0) + soft)
                stop = jnp.minimum(z, 0.0) - soft
                rest = jnp.where(past, stay, 0.0)
                hi = rest.astype(BF16)
                left = rest - hi.astype(F32)
                mid = left.astype(BF16)
                low = (left - mid.astype(F32)).astype(BF16)
                stack = jnp.concatenate([hi, mid, low], axis=0)
                sums = jnp.dot(stack, after, preferred_element_type=F32)
                within = sums[:span] + sums[span : 2 * span] + sums[2 * span :]
                local = jnp.where(past, jnp.exp(stop + within), 0.0).astype(BF16)
                part = jnp.dot(local, v_all[j][:, cols], preferred_element_type=F32)
                total = total + jnp.exp(carry) * part
                carry = carry + jnp.sum(rest, axis=1, keepdims=True)
                result += [total, carry]
            return tuple(result)

        start = (jnp.zeros((span, head), F32), jnp.zeros((span, 1), F32)) * heads
        state = lax.fori_loop(0, i + 1, one, start)
        return jnp.concatenate([state[2 * h] for h in range(heads)], axis=1).astype(BF16)

    for copy in near:
        copy.wait_recv()
    again = forwarded = 0
    for c in range(parts):
        for _ in range(2):
            forward(forwarded)
            forwarded += 1
        relay(c)
        for _ in range(2 if c else 0):
            forward_again(again)
            again += 1

    side_rows.wait_recv()

    @pl.when(jnp.logical_not(inner))
    def _():
        for q in range(2):
            for c in range(parts):
                relay_of(q, c).wait_recv()

    def hidden(g, u):
        flat = rows_in[...].reshape(ep * capacity, deep)
        gate = jnp.dot(flat, g.reshape(deep, -1), preferred_element_type=F32)
        up = jnp.dot(flat, u.reshape(deep, -1), preferred_element_type=F32)
        return (gate / (1.0 + jnp.exp(-gate)) * up).astype(BF16)

    def lower(h, d):
        return jnp.dot(h, d.reshape(-1, deep), preferred_element_type=F32)

    acc[...] = lower(hidden(g_ref[...], u_ref[...]), d_ref[...])
    for _ in range(2):
        forward_again(again)
        again += 1
        forward(forwarded)
        forwarded += 1
    acc[...] += lower(hidden(g_far[0], u_far[0]), d_far[0])
    for r in packs:
        for copy in packs[r]:
            copy.wait_recv()
    bias_rows[...] = bias_all[...].astype(F32)

    att = {}
    for r in (2, 1, 3, 0):
        dest = lax.rem(me + r, ep)
        got = attend(dest)
        if r == 0:
            att_all[me] = got
        else:
            att_send[r] = got
            att[r] = go(
                send(att_send.at[r], att_all.at[me], att_ssem.at[r], att_rsem.at[r], {"ep": dest})
            )
        if forwarded < len(chunks):
            forward(forwarded)
            forwarded += 1
        forward_again(again)
        again += 1
    third = hidden(g_far[1], u_far[1])
    for n in range(2 * cuts):
        cross[0, n].wait_recv()
        cross[1, n].wait_recv()
    last = hidden(g_far[2], u_far[2])
    while forwarded < len(chunks):
        forward(forwarded)
        forwarded += 1
    while again < len(chunks):
        forward_again(again)
        again += 1
    acc[...] += lower(third, d_far[1])
    for n in range(2 * cuts, len(chunks)):
        cross[0, n].wait_recv()
        cross[1, n].wait_recv()
    lowest = d_far[2].reshape(-1, deep)

    def final(r, c):
        piece = slice(r * capacity, (r + 1) * capacity)
        more = jnp.dot(last[piece], lowest[:, cols_of(c)], preferred_element_type=F32)
        return (acc[piece, cols_of(c)] + more).astype(BF16)

    def outer_of(q, c):
        return send(
            outer_out.at[q, :, cols_of(c)],
            outer_in.at[q, :, cols_of(c)],
            outer_send.at[q, c],
            outer_recv.at[q, c],
            {"ep": side},
        )

    for c in range(parts):
        for q in range(2):
            outer_out[q, :, cols_of(c)] = final(2 + q, c)

            @pl.when(jnp.logical_not(inner))
            def _():
                outer_of(q, c).start()

    for c in range(parts):
        back_out[:, cols_of(c)] = final(1, c)
    side_back = go(send(back_out, back_in.at[1], back_ssem, back_rsem, {"ep": side}))
    for c in range(parts):
        back_in[0, :, cols_of(c)] = final(0, c)

    def home_of(q, c):
        return send(
            dense_out.at[q, :, cols_of(c)],
            dense_back.at[:, cols_of(c)],
            home_send.at[q, c],
            home_recv.at[c],
            {"ep": far_base + q},
        )

    def return_home(c):
        @pl.when(inner)
        def _():
            for q in range(2):
                outer_of(q, c).wait_recv()
                mine = contract_rows(sel[2 * (1 + q)], outer_out[q, :, cols_of(c)])
                outer = contract_rows(sel[2 * (1 + q) + 1], outer_in[q, :, cols_of(c)])
                gate = gate_cols[1 + q]
                dense_out[q, :, cols_of(c)] = (
                    gate[:, 0:1] * mine + gate[:, 1:2] * outer
                ).astype(BF16)
                home_of(q, c).start()

    return_home(0)
    for r in att:
        att[r].wait_recv()
    ow_copy.wait()
    attended = jnp.concatenate([att_all[j] for j in range(ep)], axis=1)
    share = mixed_ref.shape[0]
    term = jnp.dot(attended, ow[...], preferred_element_type=F32).astype(BF16)
    proj[...] = term.reshape(proj.shape)
    shares = [
        go(send(proj.at[mates[m]], proj_in.at[m], proj_ssem.at[m], proj_rsem.at[m], {"tp": mates[m]}))
        for m in (2, 3, 1)
    ]
    for c in range(1, parts):
        return_home(c)
    whole = proj[tp].astype(F32)
    for copy in shares:
        copy.wait_recv()
    for m in (1, 2, 3):
        whole = whole + proj_in[m].astype(F32)
    scale = lax.rsqrt(jnp.mean(whole * whole, axis=-1, keepdims=True) + 1e-06)
    mixed_ref[...] = (whole * scale * mix_gain_ref[...]).astype(BF16)
    gate = gate_cols[0]
    side_back.wait_recv()
    for c in range(parts):
        mine = contract_rows(sel[0], back_in[0, :, cols_of(c)])
        beside = contract_rows(sel[1], back_in[1, :, cols_of(c)])
        acc[0:tokens, cols_of(c)] = gate[:, 0:1] * mine + gate[:, 1:2] * beside
    for c in range(parts):
        home_of(0, c).wait_recv()
        out_ref[:, cols_of(c)] = (
            acc[0:tokens, cols_of(c)] + dense_back[:, cols_of(c)].astype(F32)
        ).astype(BF16)
    for copy in started:
        copy.wait_send()
    for q in range(2):
        for c in range(parts):

            @pl.when(inner)
            def _():
                relay_of(q, c).wait_send()
                home_of(q, c).wait_send()

            @pl.when(jnp.logical_not(inner))
            def _():
                outer_of(q, c).wait_send()


def settle_kernel(mixed_ref, out_ref, mixed_to, out_to):
    mixed_to[...] = mixed_ref[...]
    out_to[...] = out_ref[...]


def fused_device(
    groups,
    ep,
    tp,
    queries,
    keys,
    values,
    stop_bias,
    out_weight,
    mix_gain,
    moe_input,
    ffn_gain,
    expert_ids,
    expert_scores,
    gate_weight,
    up_weight,
    down_weight,
):
    span, cols = queries.shape
    tokens, deep = moe_input.shape
    top = expert_ids.shape[1]
    capacity = 3 * tokens * top // (2 * ep)
    width = cols // ep
    heads = stop_bias.shape[1]
    units = gate_weight.shape[2]
    cuts = 4
    parts = 4
    lines = 8
    gate = gate_weight.reshape(groups, cuts, deep // (groups * cuts), units)
    up = up_weight.reshape(gate.shape)
    down = down_weight.reshape(groups, cuts, units // (groups * cuts), deep)
    chunks = 3 * cuts
    vmem = pl.BlockSpec(memory_space=pltpu.VMEM)
    dma = pltpu.SemaphoreType.DMA
    results = pl.pallas_call(
        functools.partial(layer_kernel, ep, capacity, cols // heads),
        out_shape=(
            jax.ShapeDtypeStruct((span // tp, deep), BF16),
            jax.ShapeDtypeStruct((tokens, deep), BF16),
        ),
        in_specs=[vmem] * 4 + [pl.BlockSpec(memory_space=pl.ANY)] + [vmem] * 8,
        out_specs=(vmem, vmem),
        scratch_shapes=[
            pltpu.VMEM((ep, span, width), BF16),
            pltpu.VMEM((ep, span, width), BF16),
            pltpu.VMEM((ep, span, width), BF16),
            pltpu.VMEM((ep, heads, span), BF16),
            pltpu.VMEM((ep, heads, span), F32),
            pltpu.VMEM((ep, span, width), BF16),
            pltpu.VMEM((ep, span, width), BF16),
            pltpu.VMEM((tp, span // tp, deep), BF16),
            pltpu.VMEM((tp, span // tp, deep), BF16),
            pltpu.VMEM(out_weight.shape, BF16),
            pltpu.VMEM((lines, tokens), F32),
            pltpu.VMEM((2, lines, tokens), F32),
            pltpu.VMEM((tokens, deep), BF16),
            pltpu.VMEM((2, tokens, deep), BF16),
            pltpu.VMEM((6, capacity, tokens), BF16),
            pltpu.VMEM((3, tokens, tokens), F32),
            pltpu.VMEM((capacity, deep), BF16),
            pltpu.VMEM((2, capacity, deep), BF16),
            pltpu.VMEM((ep, capacity, deep), BF16),
            pltpu.VMEM((ep * capacity, deep), F32),
            pltpu.VMEM((capacity, deep), BF16),
            pltpu.VMEM((2, capacity, deep), BF16),
            pltpu.VMEM((2, capacity, deep), BF16),
            pltpu.VMEM((2, capacity, deep), BF16),
            pltpu.VMEM((2, tokens, deep), BF16),
            pltpu.VMEM((tokens, deep), BF16),
            pltpu.VMEM((3,) + gate.shape, BF16),
            pltpu.VMEM((3,) + up.shape, BF16),
            pltpu.VMEM((3,) + down.shape, BF16),
            dma(()),
            dma((ep, 4)),
            dma((ep, 4)),
            dma(()),
            dma(()),
            dma(()),
            dma((2,)),
            dma((parts,)),
            dma((2, parts)),
            dma((2, parts)),
            dma((2, parts)),
            dma((ep,)),
            dma((ep,)),
            dma(()),
            dma(()),
            dma((2, parts)),
            dma((2, parts)),
            dma((2, parts)),
            dma((parts,)),
            dma((tp,)),
            dma((tp,)),
            dma((3,)),
            dma((3,)),
            dma((chunks,)),
            dma((chunks,)),
            dma((chunks,)),
            dma((chunks,)),
            dma((2, chunks)),
            dma((2, chunks)),
        ],
        compiler_params=pltpu.CompilerParams(
            collective_id=0, has_side_effects=True, vmem_limit_bytes=60 * 2**20
        ),
    )(
        queries,
        keys,
        values,
        stop_bias.T,
        out_weight,
        mix_gain.reshape(1, deep),
        moe_input,
        ffn_gain.reshape(1, deep),
        expert_ids.T,
        expert_scores.T,
        gate,
        up,
        down,
    )
    return pl.pallas_call(
        settle_kernel,
        out_shape=tuple(jax.ShapeDtypeStruct(r.shape, r.dtype) for r in results),
        in_specs=[vmem] * 2,
        out_specs=(vmem, vmem),
    )(*results)


def pick_plan(groups, ep, tp, *args):
    heads = args[3].shape[1]
    width = args[0].shape[1] // ep
    if groups == 2 and tp == 4 and ep == 4 and heads % ep == 0 and width % 128 == 0:
        return fused_device(groups, ep, tp, *args)
    return per_device(*args)


def solution(mesh):
    return jax.shard_map(
        functools.partial(pick_plan, mesh.shape["grp"], mesh.shape["ep"], mesh.shape["tp"]),
        mesh=mesh,
        in_specs=(
            P(("grp", "ep"), "tp"),
            P(("grp", "ep"), "tp"),
            P(("grp", "ep"), "tp"),
            P(("grp", "ep"), "tp"),
            P("tp", None),
            P(),
            P(("grp", "ep", "tp"), None),
            P(),
            P(("grp", "ep", "tp"), None),
            P(("grp", "ep", "tp"), None),
            P("ep", None, "tp"),
            P("ep", None, "tp"),
            P("ep", "tp", None),
        ),
        out_specs=(P(("grp", "ep", "tp"), None), P(("grp", "ep", "tp"), None)),
        check_vma=False,
    )
```

profile of v0, /device:TPU:0, one launch (start us, length us, event | category | flops | bytes accessed | tf_op | source)
XLA Modules:
  0.0 92.9 jit_solution(15859741015897009023)
XLA Ops:
  0.6 90.3 %shard_map.140 = (bf16[32,2048]{1,0:T(8,128)(2,1)}, bf16[128,2048]{1,0:T(8,128)(2,1)}) custom-call(bf16[128,512]{1,0:T(8,128)(2,1)} %q_ref.1, bf16[128,512]{1,0:T(8,128)(2,1)} %k_ref.1, bf16[128,512]{1,0:T(8,128)(2,1)} %v_ref.1, bf16[8,128]{1,0:T(8,128)(2,1)} %bitcast.13, bf16[512,2048]{1,0:T(8,128)(2,1)} %ow_ref.1, f32[1,2048]{1,0:T(1,128)} %bitcast.11, ...), custom_call_target="tpu_custom_call" | custom-call | tf_op jit(solution)/shard_map/pallas_call | solution.py:724
  91.0 2.0 %shard_map.141 = (bf16[32,2048]{1,0:T(8,128)(2,1)}, bf16[128,2048]{1,0:T(8,128)(2,1)}) custom-call(bf16[32,2048]{1,0:T(8,128)(2,1)} %get-tuple-element.4.mixed_ref, bf16[128,2048]{1,0:T(8,128)(2,1)} %get-tuple-element.5.out_ref), custom_call_target="tpu_custom_call" | custom-call | tf_op jit(solution)/shard_map/pallas_call | solution.py:810
where the time goes:
time: 93.1 us; the launch traced here: 92.9 us
  Pallas kernels  92.3 us (99%)
    pallas_call x1, Pallas kernels, fused_device(): pl.pallas_call(functools.partial(layer_kernel, ep, capacity, cols // head...  90.3 us
    pallas_call x1, Pallas kernels, fused_device(): pl.pallas_call(settle_kernel, out_shape=tuple((jax.ShapeDtypeStruct(r.sha...  1.96 us

commit v1 on v0

v1 whole, which is shorter than its diff:
```python
import functools

import jax
import jax.numpy as jnp
from jax import lax
from jax.experimental import pallas as pl
from jax.experimental.pallas import tpu as pltpu
from jax.sharding import PartitionSpec as P

MESH = pl.DeviceIdType.MESH
F32 = jnp.float32
BF16 = jnp.bfloat16


def norm_rows(values, gain):
    values = values.astype(jnp.float32)
    scale = lax.rsqrt(jnp.mean(values * values, axis=-1, keepdims=True) + 1e-06)
    return values * scale * gain


def break_terms(query_heads, query_place, key_block, bias_block, first):
    span = key_block.shape[0]
    heads = query_heads.shape[1]
    key_heads = key_block.reshape(span, heads, -1)
    scores = jnp.einsum("qhd,khd->hqk", query_heads, key_heads, preferred_element_type=jnp.float32)
    scores = scores * query_heads.shape[2] ** (-0.5) + bias_block.astype(jnp.float32).T[:, None, :]
    key_place = first + jnp.arange(span)
    past = (key_place[None, :] < query_place[:, None])[None]
    rest = jnp.where(past, jax.nn.log_sigmoid(-scores), 0.0)
    later = lax.cumsum(rest, axis=2, reverse=True)
    return (scores, past, rest, later)


def block_part(scores, past, rest, later, value_block, heads):
    within = later - rest
    local = jnp.where(past, jnp.exp(jax.nn.log_sigmoid(scores) + within), 0.0).astype(jnp.bfloat16)
    span = value_block.shape[0]
    value_heads = value_block.reshape(span, heads, -1)
    part = jnp.einsum("hqk,khd->qhd", local, value_heads, preferred_element_type=jnp.float32)
    return part.reshape(part.shape[0], -1)


def keep(state):
    return state


def dispatch_plan(normed, expert_ids, experts, capacity):
    rows, top = expert_ids.shape
    flat_ids = expert_ids.reshape(rows * top)
    onehot = (flat_ids[:, None] == jnp.arange(experts)[None, :]).astype(jnp.int32)
    earlier = jnp.cumsum(onehot, axis=0) - onehot
    place = jnp.sum(earlier * onehot, axis=1)
    target = flat_ids * capacity + place
    source = (
        jnp.zeros((experts * capacity,), jnp.int32)
        .at[target]
        .set(jnp.arange(rows * top, dtype=jnp.int32) // top + 1)
    )
    padded = jnp.concatenate([jnp.zeros((1, normed.shape[1]), normed.dtype), normed], axis=0)
    return (padded[source].reshape(experts, capacity, normed.shape[1]), target)


def expert_hidden(piece, gate_weight, up_weight):
    flat = piece.reshape(-1, piece.shape[-1])
    gate = jnp.dot(flat, gate_weight[0], preferred_element_type=jnp.float32)
    upward = jnp.dot(flat, up_weight[0], preferred_element_type=jnp.float32)
    hidden = (jax.nn.silu(gate) * upward).astype(jnp.bfloat16)
    return hidden.reshape(piece.shape[0], piece.shape[1], -1)


def send_back(summed):
    return lax.all_to_all(
        summed.astype(jnp.bfloat16), "ep", split_axis=0, concat_axis=0, tiled=True
    )


def return_rows(hidden_all, down_weight, sources):
    flat = hidden_all.reshape(-1, hidden_all.shape[2])
    product = jnp.dot(flat, down_weight[0], preferred_element_type=jnp.float32)
    return send_back(
        lax.psum_scatter(
            product.reshape(sources * lax.axis_size("tp"), hidden_all.shape[1], -1).astype(
                jnp.bfloat16
            ),
            "tp",
            scatter_dimension=0,
            tiled=True,
        ).astype(jnp.float32)
    )


def per_device(
    queries,
    keys,
    values,
    stop_bias,
    out_weight,
    mix_gain,
    moe_input,
    ffn_gain,
    expert_ids,
    expert_scores,
    gate_weight,
    up_weight,
    down_weight,
):
    span = queries.shape[0]
    heads = stop_bias.shape[1]
    width_heads = queries.shape[1]
    blocks = lax.axis_size("ep")
    own_first = lax.axis_index("ep") * span
    query_heads = queries.reshape(span, heads, -1)
    query_place = own_first + jnp.arange(span)

    def piece_rows(piece, index):
        return tuple((lax.dynamic_slice_in_dim(member, index * span, span, 0) for member in piece))

    start_state = (
        jnp.zeros((blocks, heads, span), jnp.float32),
        jnp.zeros((blocks, span, width_heads), jnp.float32),
    )
    piece = (
        lax.all_gather(keys, "ep", axis=0, tiled=True),
        lax.all_gather(values, "ep", axis=0, tiled=True),
        lax.all_gather(stop_bias, "ep", axis=0, tiled=True),
    )

    def one_block(index, state):
        key_block, value_block, bias_block = piece_rows(piece, index)
        first = index * span

        def compute(inner_state):
            totals, parts = inner_state
            scores, past, rest, later = break_terms(
                query_heads, query_place, key_block, bias_block, first
            )
            part = block_part(scores, past, rest, later, value_block, heads)
            number = first // span
            totals = lax.dynamic_update_index_in_dim(totals, later[:, :, 0], number, 0)
            parts = lax.dynamic_update_index_in_dim(parts, part, number, 0)
            return (totals, parts)

        return lax.cond(first <= own_first, compute, keep, state)

    totals, parts = lax.fori_loop(0, piece[0].shape[0] // span, one_block, start_state)
    carried = lax.cumsum(totals, axis=0, reverse=True) - totals
    factor = jnp.exp(carried).transpose(0, 2, 1)[:, :, :, None]
    attended = jnp.sum(factor * parts.reshape(blocks, span, heads, -1), axis=0).reshape(
        span, width_heads
    )
    attended = attended.astype(jnp.bfloat16)
    projected = lax.psum_scatter(
        jnp.dot(attended, out_weight, preferred_element_type=jnp.float32).astype(jnp.bfloat16),
        "tp",
        scatter_dimension=0,
        tiled=True,
    ).astype(jnp.float32)
    mixed = norm_rows(projected, mix_gain).astype(jnp.bfloat16)
    normed = norm_rows(moe_input, ffn_gain).astype(jnp.bfloat16)
    rows, top = expert_ids.shape
    experts = lax.axis_size("ep")
    capacity = 3 * rows * top // (2 * experts)
    weights = expert_scores / jnp.sum(expert_scores, axis=1, keepdims=True)
    outbound, target = dispatch_plan(normed, expert_ids, experts, capacity)
    arrived = lax.all_to_all(outbound, "ep", split_axis=0, concat_axis=0, tiled=True)
    hidden_all = expert_hidden(
        lax.all_gather(arrived, "tp", axis=0, tiled=True), gate_weight, up_weight
    )
    returned = return_rows(hidden_all, down_weight, arrived.shape[0])
    picked = returned.reshape(experts * capacity, -1)[target].reshape(rows, top, -1)
    experts_mixed = jnp.sum(picked.astype(jnp.float32) * weights[:, :, None], axis=1).astype(
        jnp.bfloat16
    )
    return (mixed, experts_mixed)


def layer_kernel(
    ep,
    capacity,
    head,
    q_ref,
    k_ref,
    v_ref,
    bias_ref,
    ow_ref,
    mix_gain_ref,
    x_ref,
    ffn_gain_ref,
    ids_ref,
    scores_ref,
    g_ref,
    u_ref,
    d_ref,
    mixed_ref,
    out_ref,
    x_own,
    gain_own,
    mix_own,
    ids_own,
    scores_own,
    qkv_all,
    bias_all,
    bias_rows,
    att_send,
    att_all,
    proj,
    proj_in,
    ow,
    meta,
    meta_in,
    normed_ref,
    dense_in,
    sel,
    sel_back,
    gate_cols,
    outbound,
    relay_out,
    rows_in,
    hid,
    acc,
    back_out,
    back_in,
    outer_out,
    outer_in,
    dense_out,
    dense_back,
    g_all,
    u_all,
    d_all,
    load_sem,
    own_sem,
    ow_sem,
    pack_send,
    pack_recv,
    bias_send,
    bias_recv,
    row_send,
    row_recv,
    meta_send,
    meta_recv,
    dense_send,
    dense_recv,
    relay_send,
    relay_recv,
    att_ssem,
    att_rsem,
    back_ssem,
    back_rsem,
    outer_send,
    outer_recv,
    home_send,
    home_recv,
    proj_ssem,
    proj_rsem,
    near_send,
    near_recv,
    x_send,
    x_recv,
    y_send,
    y_recv,
    cross_send,
    cross_wide,
    cross_down,
):
    me = lax.axis_index("ep")
    tp = lax.axis_index("tp")
    grp = lax.axis_index("grp")
    chip, core = tp // 2, tp % 2
    mates = [None, chip * 2 + (1 - core), (1 - chip) * 2 + core, (1 - chip) * 2 + (1 - core)]
    span = q_ref.shape[0]
    width = qkv_all.shape[3]
    heads = width // head
    tokens, deep = x_ref.shape
    top = ids_ref.shape[0]
    parts = dense_recv.shape[1]
    fine = home_recv.shape[0]
    wide_cuts = 2 * g_ref.shape[1]

    half = me // 2
    is_inner = lax.rem(me + 1, ep) // 2
    inner = is_inner == 1
    outside = is_inner == 0
    side = me + 1 - 2 * (me % 2)
    far = (3 * (1 - half), 2 - half)

    loads = [
        pltpu.make_async_copy(s, t, load_sem.at[n])
        for n, (s, t) in enumerate(
            (
                (x_ref, x_own),
                (ids_ref, ids_own),
                (scores_ref, scores_own),
                (ffn_gain_ref, gain_own),
                (g_ref, g_all.at[0]),
                (u_ref, u_all.at[0]),
                (d_ref, d_all.at[0]),
                (mix_gain_ref, mix_own),
                (bias_ref, bias_all.at[me]),
            )
        )
    ]
    own = pl.ds(pl.multiple_of(me * width, width), width)
    mine = [
        pltpu.make_async_copy(r.at[:, own], qkv_all.at[me, n], own_sem.at[n])
        for n, r in enumerate((q_ref, k_ref, v_ref))
    ]
    ow_copy = pltpu.make_async_copy(ow_ref, ow, ow_sem)
    for copy in loads:
        copy.start()

    barrier = pltpu.get_barrier_semaphore()
    peers = [{"ep": lax.rem(me + r, ep)} for r in range(1, ep)]
    peers += [{"tp": mates[m]} for m in (1, 2, 3)] + [{"grp": 1 - grp}]
    for peer in peers:
        pl.semaphore_signal(barrier, inc=1, device_id=peer, device_id_type=MESH)
    for copy in mine:
        copy.start()
    ow_copy.start()

    def send(src, dst, ssem, rsem, peer):
        return pltpu.make_async_remote_copy(
            src_ref=src,
            dst_ref=dst,
            send_sem=ssem,
            recv_sem=rsem,
            device_id=peer,
            device_id_type=MESH,
        )

    mate = {"tp": mates[1]}

    def arrived(ref, sem):
        send(ref, ref, sem, sem, mate).wait_recv()

    def drained(ref, sem):
        send(ref, ref, sem, sem, mate).wait_send()

    def cols_of(c, n=parts):
        return slice(c * (deep // n), (c + 1) * (deep // n))

    def piece_of(n, s, g):
        if n < wide_cuts:
            return (g_all, u_all)[n % 2].at[s, g, n // 2]
        return d_all.at[s, g, :, cols_of(n - wide_cuts, fine)]

    def kind_of(n):
        return n % 2 if n < wide_cuts else 2

    chunks = wide_cuts + fine

    for n in range(4):
        loads[n].wait()
    gates = scores_own[...]
    gates = gates / jnp.sum(gates, axis=0, keepdims=True)
    meta[...] = jnp.zeros_like(meta)
    meta[0:top] = ids_own[...].astype(F32)
    meta[top : 2 * top] = gates
    values = x_own[...].astype(F32)
    scale = lax.rsqrt(jnp.mean(values * values, axis=-1, keepdims=True) + 1e-06)
    normed_ref[...] = (values * scale * gain_own[...]).astype(BF16)

    pl.semaphore_wait(barrier, len(peers))

    def over_x(n):
        return send(
            piece_of(n, 0, grp),
            piece_of(n, 2, grp),
            x_send.at[kind_of(n)],
            x_recv.at[n],
            {"tp": mates[2]},
        )

    loads[4].wait()
    over_x(0).start()
    send(meta, meta_in.at[is_inner], meta_send, meta_recv.at[is_inner], {"ep": far[1]}).start()

    def dense_of(slot, c):
        return send(
            normed_ref.at[:, cols_of(c)],
            dense_in.at[slot, :, cols_of(c)],
            dense_send,
            dense_recv.at[slot, c],
            {"ep": far[1]},
        )

    for c in range(parts):
        dense_of(is_inner, c).start()
    loads[5].wait()
    for n in range(1, wide_cuts):
        over_x(n).start()
    loads[6].wait()
    for n in range(wide_cuts, chunks):
        over_x(n).start()
    nears = [
        send(r.at[0], r.at[1], near_send.at[n], near_recv.at[n], mate)
        for n, r in enumerate((g_all, u_all, d_all))
    ]
    for copy in nears:
        copy.start()

    square = (tokens, tokens)
    lane = lax.broadcasted_iota(jnp.int32, square, 1)
    sub = lax.broadcasted_iota(jnp.int32, square, 0)
    earlier = (sub < lane).astype(BF16)
    slots = lax.broadcasted_iota(jnp.int32, (capacity, tokens), 0).astype(F32)

    def route(table, at):
        named = jnp.zeros(square, F32)
        gate = jnp.zeros(square, F32)
        for n, e in enumerate((me, side)):
            place_of = e.astype(F32)
            for k in range(top):
                hit = table[k : k + 1, :] == place_of
                here = sub == n
                named = named + jnp.where(here & hit, 1.0, 0.0)
                gate = gate + jnp.where(here & hit, table[top + k : top + k + 1, :], 0.0)
        place = jnp.dot(named.astype(BF16), earlier, preferred_element_type=F32)
        for n in range(2):
            chosen = jnp.where(slots == place[n : n + 1, :], named[n : n + 1, :], 0.0)
            sel[at, n * capacity : (n + 1) * capacity] = chosen.astype(BF16)
            sel_back[2 * at + n] = chosen.T.astype(BF16)
        gate_cols[at] = gate.T

    def pick(at, block):
        return jnp.dot(sel[at], block, preferred_element_type=F32).astype(BF16)

    route(meta[...], 0)
    for c in range(parts):
        both = pick(0, normed_ref[:, cols_of(c)])
        rows_in[0, :, cols_of(c)] = both[:capacity]
        outbound[:, cols_of(c)] = both[capacity:]
    side_rows = send(outbound, rows_in.at[1], row_send, row_recv, {"ep": side})
    side_rows.start()

    def relay_of(slot, c):
        return send(
            relay_out.at[slot, :, cols_of(c)],
            rows_in.at[2 + slot, :, cols_of(c)],
            relay_send.at[slot],
            relay_recv.at[slot],
            {"ep": side},
        )

    def relay(slot, c):
        @pl.when(inner)
        def _():
            dense_of(slot, c).wait_recv()
            both = pick(1 + slot, dense_in[slot, :, cols_of(c)])
            relay_out[slot, :, cols_of(c)] = both[capacity:]
            relay_of(slot, c).start()
            rows_in[2 + slot, :, cols_of(c)] = both[:capacity]

    def forward(n):
        over_x(n).wait_recv()
        send(
            piece_of(n, 2, grp),
            piece_of(n, 2, grp),
            y_send.at[kind_of(n)],
            y_recv.at[n],
            {"grp": 1 - grp},
        ).start()
        cross_of(0, n).start()

    def cross_of(way, n):
        g = grp if way == 0 else 1 - grp
        landed = cross_wide.at[way, n % 2] if n < wide_cuts else cross_down.at[way, n - wide_cuts]
        return send(piece_of(n, 2, g), piece_of(n, 3, g), cross_send.at[way, kind_of(n)], landed, mate)

    def forward_again(n):
        arrived(piece_of(n, 2, 1 - grp), y_recv.at[n])
        cross_of(1, n).start()

    units = hid.shape[1] // 4

    def hidden(s, flat, rows):
        gate = jnp.dot(flat, g_all[s].reshape(deep, units), preferred_element_type=F32)
        up = jnp.dot(flat, u_all[s].reshape(deep, units), preferred_element_type=F32)
        hid[rows, s * units : (s + 1) * units] = (gate / (1.0 + jnp.exp(-gate)) * up).astype(BF16)

    early = 3 * capacity

    def hidden_early(s):
        hidden(s, rows_in[0:3].reshape(early, deep), slice(0, early))

    def hidden_late(s):
        hidden(s, rows_in[3], slice(early, early + capacity))

    relays = 2 * parts
    lag = 3
    when = {}
    for m in range(relays):
        when[2 * m + (2 if m < parts else 1)] = m

    for n in range(wide_cuts):
        if n in when:
            relay(when[n] // parts, when[n] % parts)
        forward(n)
        if n == 1:

            @pl.when(inner)
            def _():
                for slot in range(2):
                    arrived(meta_in.at[slot], meta_recv.at[slot])
                    route(meta_in[slot], 1 + slot)

        if n >= lag:
            forward_again(n - lag)

    pieces = (q_ref, k_ref, v_ref)
    dests = (
        far[1] * is_inner + side * (1 - is_inner),
        far[0] * is_inner + far[1] * (1 - is_inner),
        side * is_inner + far[0] * (1 - is_inner),
    )
    for r, dest in enumerate(dests):
        cols = pl.ds(pl.multiple_of(dest * width, width), width)
        for n in range(3):
            send(
                pieces[n].at[:, cols],
                qkv_all.at[me, n],
                pack_send,
                pack_recv.at[me],
                {"ep": dest},
            ).start()
        send(bias_ref, bias_all.at[me], bias_send.at[r], bias_recv.at[me], {"ep": dest}).start()

    side_rows.wait_recv()

    @pl.when(outside)
    def _():
        arrived(relay_out.at[0], relay_recv.at[0])

    hidden_early(0)
    forward_again(wide_cuts - 3)
    forward(wide_cuts)
    for copy in nears:
        copy.wait_recv()
    hidden_early(1)
    forward_again(wide_cuts - 2)
    forward(wide_cuts + 1)
    forward_again(wide_cuts - 1)
    hidden_early(2)
    forward(wide_cuts + 2)
    forward_again(wide_cuts)

    @pl.when(outside)
    def _():
        arrived(relay_out.at[1], relay_recv.at[1])

    for s in range(3):
        hidden_late(s)
    forward(wide_cuts + 3)
    forward_again(wide_cuts + 1)
    for n, r in enumerate((g_all, u_all)):
        arrived(r.at[3, grp], cross_wide.at[0, n])
        arrived(r.at[3, 1 - grp], cross_wide.at[1, n])
    hidden_early(3)
    hidden_late(3)

    def outer_of(c):
        cols = cols_of(c, fine)
        return send(
            outer_out.at[:, :, cols], outer_in.at[:, :, cols], outer_send, outer_recv.at[c], {"ep": side}
        )

    def final(c):
        cols = cols_of(c, fine)
        for way in range(2):
            cross_of(way, wide_cuts + c).wait_recv()
        down = jnp.concatenate(
            [d_all[s, :, :, cols].reshape(units, deep // fine) for s in range(4)], axis=0
        )
        whole = jnp.dot(hid[...], down, preferred_element_type=F32).astype(BF16)
        for slot in range(2):
            first = (2 + slot) * capacity
            outer_out[slot, :, cols] = whole[first : first + capacity]

        @pl.when(outside)
        def _():
            outer_of(c).start()

        back_out[:, cols] = whole[capacity : 2 * capacity]
        back_in[0, :, cols] = whole[:capacity]

    def home_of(slot, c):
        return send(
            dense_out.at[slot, :, cols_of(c, fine)],
            dense_back.at[:, cols_of(c, fine)],
            home_send.at[slot],
            home_recv.at[c],
            {"ep": far[slot]},
        )

    def weigh(at, near_rows, far_rows):
        gate = gate_cols[at]
        here = jnp.dot(sel_back[2 * at], near_rows, preferred_element_type=F32)
        there = jnp.dot(sel_back[2 * at + 1], far_rows, preferred_element_type=F32)
        return gate[:, 0:1] * here + gate[:, 1:2] * there

    def return_home(c):
        cols = cols_of(c, fine)

        @pl.when(inner)
        def _():
            outer_of(c).wait_recv()
            for slot in range(2):
                dense_out[slot, :, cols] = weigh(
                    1 + slot, outer_out[slot, :, cols], outer_in[slot, :, cols]
                ).astype(BF16)
                home_of(slot, c).start()

    block = (span, span)
    key_sub = lax.broadcasted_iota(jnp.int32, block, 0)
    key_lane = lax.broadcasted_iota(jnp.int32, block, 1)
    after = (key_sub > key_lane).astype(BF16)
    past = key_lane < key_sub

    def attend(i):
        result = []
        for h in range(heads):
            cols = slice(h * head, (h + 1) * head)
            query = qkv_all[i, 0][:, cols]
            for j in range(i, -1, -1):
                z = lax.dot_general(
                    query,
                    qkv_all[j, 1][:, cols],
                    (((1,), (1,)), ((), ())),
                    preferred_element_type=F32,
                )
                z = z * head ** (-0.5) + bias_rows[j, pl.ds(me * heads + h, 1), :]
                soft = jnp.log1p(jnp.exp(-jnp.abs(z)))
                rest = -(jnp.maximum(z, 0.0) + soft)
                stop = jnp.minimum(z, 0.0) - soft
                if j == i:
                    rest = jnp.where(past, rest, 0.0)
                hi = rest.astype(BF16)
                left = rest - hi.astype(F32)
                mid = left.astype(BF16)
                low = (left - mid.astype(F32)).astype(BF16)
                sums = jnp.dot(
                    jnp.concatenate([hi, mid, low], axis=0), after, preferred_element_type=F32
                )
                within = sums[:span] + sums[span : 2 * span] + sums[2 * span :]
                local = jnp.exp(stop + within)
                if j == i:
                    local = jnp.where(past, local, 0.0)
                part = jnp.dot(
                    local.astype(BF16), qkv_all[j, 2][:, cols], preferred_element_type=F32
                )
                total = part if j == i else total + jnp.exp(carry) * part
                if j > 0:
                    tally = jnp.sum(rest, axis=1, keepdims=True)
                    carry = tally if j == i else carry + tally
            result.append(total)
        got = jnp.concatenate(result, axis=1).astype(BF16)
        att_send[i] = got

        @pl.when(me == i)
        def _():
            att_all[i] = got

        @pl.when(me != i)
        def _():
            att_of(i, me).start()

    def att_of(i, j):
        return send(att_send.at[i], att_all.at[j], att_ssem.at[i], att_rsem.at[j], {"ep": i})

    final(0)
    forward(wide_cuts + 4)
    forward_again(wide_cuts + 2)
    final(1)
    forward(wide_cuts + 5)
    forward_again(wide_cuts + 3)
    final(2)
    forward(wide_cuts + 6)
    forward_again(wide_cuts + 4)
    final(3)
    for copy in mine:
        copy.wait()
    loads[8].wait()
    for r in range(1, ep):
        source = lax.rem(me + r, ep)
        arrived(qkv_all.at[source], pack_recv.at[source])
        arrived(bias_all.at[source], bias_recv.at[source])
    bias_rows[...] = bias_all[...].astype(F32)
    return_home(0)
    attend(3)
    forward(wide_cuts + 7)
    forward_again(wide_cuts + 5)
    final(4)
    return_home(1)
    attend(2)
    forward_again(wide_cuts + 6)
    final(5)
    return_home(2)
    attend(1)
    forward_again(wide_cuts + 7)
    final(6)
    return_home(3)
    attend(0)
    final(7)
    side_back = send(back_out, back_in.at[1], back_ssem, back_rsem, {"ep": side})
    side_back.start()
    for c in range(4, fine):
        return_home(c)
    for j in range(ep):

        @pl.when(me != j)
        def _():
            arrived(att_all.at[j], att_rsem.at[j])

    ow_copy.wait()
    attended = jnp.concatenate([att_all[j] for j in range(ep)], axis=1)
    term = jnp.dot(attended, ow[...], preferred_element_type=F32).astype(BF16)
    proj[...] = term.reshape(proj.shape)
    shares = [
        send(proj.at[mates[m]], proj_in.at[m], proj_ssem.at[m], proj_rsem.at[m], {"tp": mates[m]})
        for m in (2, 3, 1)
    ]
    for copy in shares:
        copy.start()
    whole = proj[tp].astype(F32)
    for copy in shares:
        copy.wait_recv()
    for m in (1, 2, 3):
        whole = whole + proj_in[m].astype(F32)
    loads[7].wait()
    scale = lax.rsqrt(jnp.mean(whole * whole, axis=-1, keepdims=True) + 1e-06)
    mixed_ref[...] = (whole * scale * mix_own[...]).astype(BF16)
    drained(normed_ref, dense_send)
    for n, r in enumerate((g_all, u_all, d_all)):
        drained(r.at[0, grp], x_send.at[n])
        drained(r.at[2, grp], y_send.at[n])
        drained(r.at[2, grp], cross_send.at[0, n])
        drained(r.at[2, 1 - grp], cross_send.at[1, n])
        nears[n].wait_send()
    drained(qkv_all.at[pl.ds(0, 3)], pack_send)
    for r in range(ep - 1):
        drained(bias_all.at[0], bias_send.at[r])
    side_rows.wait_send()
    drained(meta, meta_send)
    for i in range(ep):

        @pl.when(me != i)
        def _():
            drained(att_send.at[i], att_ssem.at[i])

    for copy in shares:
        copy.wait_send()
    side_back.wait_recv()
    for c in range(fine):
        cols = cols_of(c, fine)
        acc[:, cols] = weigh(0, back_in[0, :, cols], back_in[1, :, cols])
    side_back.wait_send()

    @pl.when(outside)
    def _():
        drained(outer_out, outer_send)

    for c in range(fine):
        cols = cols_of(c, fine)
        home_of(0, c).wait_recv()
        out_ref[:, cols] = (acc[:, cols] + dense_back[:, cols].astype(F32)).astype(BF16)

    @pl.when(inner)
    def _():
        for slot in range(2):
            drained(relay_out.at[slot], relay_send.at[slot])
            drained(dense_out.at[slot], home_send.at[slot])


def settle_kernel(mixed_ref, out_ref, mixed_to, out_to, sems):
    copies = [
        pltpu.make_async_copy(out_ref, out_to, sems.at[0]),
        pltpu.make_async_copy(mixed_ref, mixed_to, sems.at[1]),
    ]
    for copy in copies:
        copy.start()
    for copy in copies:
        copy.wait()


def fused_device(
    groups,
    ep,
    tp,
    queries,
    keys,
    values,
    stop_bias,
    out_weight,
    mix_gain,
    moe_input,
    ffn_gain,
    expert_ids,
    expert_scores,
    gate_weight,
    up_weight,
    down_weight,
):
    span, cols = queries.shape
    tokens, deep = moe_input.shape
    top = expert_ids.shape[1]
    capacity = 3 * tokens * top // (2 * ep)
    width = cols // ep
    heads = stop_bias.shape[1]
    units = gate_weight.shape[2]
    cuts = 8
    parts = 4
    fine = 8
    lines = 8
    gate = gate_weight.reshape(groups, cuts, deep // (groups * cuts), units)
    up = up_weight.reshape(gate.shape)
    down = down_weight.reshape(groups, units // groups, deep)
    chunks = 2 * cuts + fine
    vmem = pl.BlockSpec(memory_space=pltpu.VMEM)
    hbm = pl.BlockSpec(memory_space=pl.ANY)
    dma = pltpu.SemaphoreType.DMA
    results = pl.pallas_call(
        functools.partial(layer_kernel, ep, capacity, cols // heads),
        out_shape=(
            pltpu.VMEM((span // tp, deep), BF16),
            pltpu.VMEM((tokens, deep), BF16),
        ),
        in_specs=[hbm] * 13,
        out_specs=(vmem, vmem),
        scratch_shapes=[
            pltpu.VMEM((tokens, deep), BF16),
            pltpu.VMEM((1, deep), F32),
            pltpu.VMEM((1, deep), F32),
            pltpu.VMEM((top, tokens), jnp.int32),
            pltpu.VMEM((top, tokens), F32),
            pltpu.VMEM((ep, 3, span, width), BF16),
            pltpu.VMEM((ep, heads, span), BF16),
            pltpu.VMEM((ep, heads, span), F32),
            pltpu.VMEM((ep, span, width), BF16),
            pltpu.VMEM((ep, span, width), BF16),
            pltpu.VMEM((tp, span // tp, deep), BF16),
            pltpu.VMEM((tp, span // tp, deep), BF16),
            pltpu.VMEM(out_weight.shape, BF16),
            pltpu.VMEM((lines, tokens), F32),
            pltpu.VMEM((2, lines, tokens), F32),
            pltpu.VMEM((tokens, deep), BF16),
            pltpu.VMEM((2, tokens, deep), BF16),
            pltpu.VMEM((3, 2 * capacity, tokens), BF16),
            pltpu.VMEM((6, tokens, capacity), BF16),
            pltpu.VMEM((3, tokens, tokens), F32),
            pltpu.VMEM((capacity, deep), BF16),
            pltpu.VMEM((2, capacity, deep), BF16),
            pltpu.VMEM((ep, capacity, deep), BF16),
            pltpu.VMEM((ep * capacity, tp * units), BF16),
            pltpu.VMEM((tokens, deep), F32),
            pltpu.VMEM((capacity, deep), BF16),
            pltpu.VMEM((2, capacity, deep), BF16),
            pltpu.VMEM((2, capacity, deep), BF16),
            pltpu.VMEM((2, capacity, deep), BF16),
            pltpu.VMEM((2, tokens, deep), BF16),
            pltpu.VMEM((tokens, deep), BF16),
            pltpu.VMEM((4,) + gate.shape, BF16),
            pltpu.VMEM((4,) + up.shape, BF16),
            pltpu.VMEM((4,) + down.shape, BF16),
            dma((9,)),
            dma((3,)),
            dma(()),
            dma(()),
            dma((ep,)),
            dma((ep,)),
            dma((ep,)),
            dma(()),
            dma(()),
            dma(()),
            dma((2,)),
            dma(()),
            dma((2, parts)),
            dma((2,)),
            dma((2,)),
            dma((ep,)),
            dma((ep,)),
            dma(()),
            dma(()),
            dma(()),
            dma((fine,)),
            dma((2,)),
            dma((fine,)),
            dma((tp,)),
            dma((tp,)),
            dma((3,)),
            dma((3,)),
            dma((3,)),
            dma((chunks,)),
            dma((3,)),
            dma((chunks,)),
            dma((2, 3)),
            dma((2, 2)),
            dma((2, fine)),
        ],
        compiler_params=pltpu.CompilerParams(
            collective_id=0, has_side_effects=True, vmem_limit_bytes=60 * 2**20
        ),
    )(
        queries,
        keys,
        values,
        stop_bias.T,
        out_weight,
        mix_gain.reshape(1, deep),
        moe_input,
        ffn_gain.reshape(1, deep),
        expert_ids.T,
        expert_scores.T,
        gate,
        up,
        down,
    )
    results = [pltpu.with_memory_space_constraint(r, pltpu.VMEM) for r in results]
    return pl.pallas_call(
        settle_kernel,
        out_shape=tuple(jax.ShapeDtypeStruct(r.shape, r.dtype) for r in results),
        in_specs=[vmem] * 2,
        out_specs=(hbm, hbm),
        scratch_shapes=[dma((2,))],
    )(*results)


def pick_plan(groups, ep, tp, *args):
    heads = args[3].shape[1]
    width = args[0].shape[1] // ep
    if groups == 2 and tp == 4 and ep == 4 and heads % ep == 0 and width % 128 == 0:
        return fused_device(groups, ep, tp, *args)
    return per_device(*args)


def solution(mesh):
    return jax.shard_map(
        functools.partial(pick_plan, mesh.shape["grp"], mesh.shape["ep"], mesh.shape["tp"]),
        mesh=mesh,
        in_specs=(
            P(("grp", "ep"), "tp"),
            P(("grp", "ep"), "tp"),
            P(("grp", "ep"), "tp"),
            P(("grp", "ep"), "tp"),
            P("tp", None),
            P(),
            P(("grp", "ep", "tp"), None),
            P(),
            P(("grp", "ep", "tp"), None),
            P(("grp", "ep", "tp"), None),
            P("ep", None, "tp"),
            P("ep", None, "tp"),
            P("ep", "tp", None),
        ),
        out_specs=(P(("grp", "ep", "tp"), None), P(("grp", "ep", "tp"), None)),
        check_vma=False,
    )
```

time: 93.1 us -> 77.4 us (0.83)
  Pallas kernels: 92.3 us -> 76.6 us
    pallas_call x1, Pallas kernels: 90.3 us -> 75.7 us  [fused_device(): pl.pallas_call(functools.partial(layer_kernel, ep, capacity, cols // head...]
    pallas_call x1, Pallas kernels: 1.96 us -> 0.85 us  [fused_device(): pl.pallas_call(settle_kernel, out_shape=tuple((jax.ShapeDtypeStruct(r.sha...]
where the time goes in v1:
time: 77.4 us; the launch traced here: 77.2 us
  Pallas kernels  76.6 us (99%)
    pallas_call x1, Pallas kernels, fused_device(): pl.pallas_call(functools.partial(layer_kernel, ep, capacity, cols // head...  75.7 us

profile of v1, /device:TPU:0, one launch (start us, length us, event | category | flops | bytes accessed | tf_op | source)
XLA Modules:
  0.0 77.2 jit_solution(12143579100666171886)
XLA Ops:
  0.6 75.7 %shard_map.140 = (bf16[32,2048]{1,0:T(8,128)(2,1)S(1)}, bf16[128,2048]{1,0:T(8,128)(2,1)S(1)}) custom-call(bf16[128,512]{1,0:T(8,128)(2,1)} %q_ref.1, bf16[128,512]{1,0:T(8,128)(2,1)} %k_ref.1, bf16[128,512]{1,0:T(8,128)(2,1)} %v_ref.1, bf16[8,128]{1,0:T(8,128)(2,1)} %bitcast.13, bf16[512,2048]{1,0:T(8,128)(2,1)} %ow_ref.1, f32[1,2048]{1,0:T(1,128)} %bitcast.11, ...), custom_call_target="tpu_custom_call" | custom-call | tf_op jit(solution)/shard_map/pallas_call | solution.py:820
  76.4 0.8 %shard_map.141 = (bf16[32,2048]{1,0:T(8,128)(2,1)}, bf16[128,2048]{1,0:T(8,128)(2,1)}) custom-call(bf16[32,2048]{1,0:T(8,128)(2,1)S(1)} %get-tuple-element.4.mixed_ref, bf16[128,2048]{1,0:T(8,128)(2,1)S(1)} %get-tuple-element.5.out_ref), custom_call_target="tpu_custom_call" | custom-call | tf_op jit(solution)/shard_map/pallas_call | solution.py:917

commit v2 on v1

--- a/solution.py
+++ b/solution.py
@@ -217,6 +217,7 @@
     relay_out,
     rows_in,
     hid,
+    sofar,
     acc,
     back_out,
     back_in,
@@ -335,13 +336,18 @@
     def drained(ref, sem):
         send(ref, ref, sem, sem, mate).wait_send()
 
-    def cols_of(c, n=parts):
-        return slice(c * (deep // n), (c + 1) * (deep // n))
+    def cols_of(c):
+        return slice(c * (deep // parts), (c + 1) * (deep // parts))
+
+    def strip(c):
+        unit = deep // (2 * (fine - 1))
+        edges = [0, 1] + [2 * n for n in range(1, fine)]
+        return slice(edges[c] * unit, edges[c + 1] * unit)
 
     def piece_of(n, s, g):
         if n < wide_cuts:
             return (g_all, u_all)[n % 2].at[s, g, n // 2]
-        return d_all.at[s, g, :, cols_of(n - wide_cuts, fine)]
+        return d_all.at[s, g, :, strip(n - wide_cuts)]
 
     def kind_of(n):
         return n % 2 if n < wide_cuts else 2
@@ -383,8 +389,34 @@
             {"ep": far[1]},
         )
 
+    pieces = (q_ref, k_ref, v_ref)
+
+    def pack(r, dest):
+        cols = pl.ds(pl.multiple_of(dest * width, width), width)
+        for n in range(3):
+            send(
+                pieces[n].at[:, cols],
+                qkv_all.at[me, n],
+                pack_send,
+                pack_recv.at[me],
+                {"ep": dest},
+            ).start()
+        send(bias_ref, bias_all.at[me], bias_send.at[r], bias_recv.at[me], {"ep": dest}).start()
+
+    @pl.when(inner)
+    def _():
+        pack(0, far[1])
+        pack(1, far[0])
+
     for c in range(parts):
         dense_of(is_inner, c).start()
+
+    @pl.when(outside)
+    def _():
+        pack(0, far[1])
+        pack(1, far[0])
+        pack(2, side)
+
     loads[5].wait()
     for n in range(1, wide_cuts):
         over_x(n).start()
@@ -395,9 +427,6 @@
         send(r.at[0], r.at[1], near_send.at[n], near_recv.at[n], mate)
         for n, r in enumerate((g_all, u_all, d_all))
     ]
-    for copy in nears:
-        copy.start()
-
     square = (tokens, tokens)
     lane = lax.broadcasted_iota(jnp.int32, square, 1)
     sub = lax.broadcasted_iota(jnp.int32, square, 0)
@@ -444,6 +473,9 @@
     def relay(slot, c):
         @pl.when(inner)
         def _():
+            if c == 0:
+                arrived(meta_in.at[slot], meta_recv.at[slot])
+                route(meta_in[slot], 1 + slot)
             dense_of(slot, c).wait_recv()
             both = pick(1 + slot, dense_in[slot, :, cols_of(c)])
             relay_out[slot, :, cols_of(c)] = both[capacity:]
@@ -463,7 +495,7 @@
 
     def cross_of(way, n):
         g = grp if way == 0 else 1 - grp
-        landed = cross_wide.at[way, n % 2] if n < wide_cuts else cross_down.at[way, n - wide_cuts]
+        landed = cross_wide.at[way, n % 2] if n < wide_cuts else cross_down.at[n - wide_cuts]
         return send(piece_of(n, 2, g), piece_of(n, 3, g), cross_send.at[way, kind_of(n)], landed, mate)
 
     def forward_again(n):
@@ -472,142 +504,41 @@
 
     units = hid.shape[1] // 4
 
-    def hidden(s, flat, rows):
+    depth = deep // 2
+
+    def rows_of(a, b):
+        return slice(a * capacity, b * capacity)
+
+    def activate(gate, up, s, rows):
+        hid[rows, s * units : (s + 1) * units] = (gate / (1.0 + jnp.exp(-gate)) * up).astype(BF16)
+
+    def hidden(s, a, b):
+        flat = rows_in[a:b].reshape((b - a) * capacity, deep)
         gate = jnp.dot(flat, g_all[s].reshape(deep, units), preferred_element_type=F32)
         up = jnp.dot(flat, u_all[s].reshape(deep, units), preferred_element_type=F32)
-        hid[rows, s * units : (s + 1) * units] = (gate / (1.0 + jnp.exp(-gate)) * up).astype(BF16)
-
-    early = 3 * capacity
+        activate(gate, up, s, rows_of(a, b))
 
     def hidden_early(s):
-        hidden(s, rows_in[0:3].reshape(early, deep), slice(0, early))
+        hidden(s, 0, 3)
 
     def hidden_late(s):
-        hidden(s, rows_in[3], slice(early, early + capacity))
-
-    relays = 2 * parts
-    lag = 3
-    when = {}
-    for m in range(relays):
-        when[2 * m + (2 if m < parts else 1)] = m
-
-    for n in range(wide_cuts):
-        if n in when:
-            relay(when[n] // parts, when[n] % parts)
-        forward(n)
-        if n == 1:
-
-            @pl.when(inner)
-            def _():
-                for slot in range(2):
-                    arrived(meta_in.at[slot], meta_recv.at[slot])
-                    route(meta_in[slot], 1 + slot)
-
-        if n >= lag:
-            forward_again(n - lag)
-
-    pieces = (q_ref, k_ref, v_ref)
-    dests = (
-        far[1] * is_inner + side * (1 - is_inner),
-        far[0] * is_inner + far[1] * (1 - is_inner),
-        side * is_inner + far[0] * (1 - is_inner),
-    )
-    for r, dest in enumerate(dests):
-        cols = pl.ds(pl.multiple_of(dest * width, width), width)
-        for n in range(3):
-            send(
-                pieces[n].at[:, cols],
-                qkv_all.at[me, n],
-                pack_send,
-                pack_recv.at[me],
-                {"ep": dest},
-            ).start()
-        send(bias_ref, bias_all.at[me], bias_send.at[r], bias_recv.at[me], {"ep": dest}).start()
-
-    side_rows.wait_recv()
-
-    @pl.when(outside)
-    def _():
-        arrived(relay_out.at[0], relay_recv.at[0])
-
-    hidden_early(0)
-    forward_again(wide_cuts - 3)
-    forward(wide_cuts)
-    for copy in nears:
-        copy.wait_recv()
-    hidden_early(1)
-    forward_again(wide_cuts - 2)
-    forward(wide_cuts + 1)
-    forward_again(wide_cuts - 1)
-    hidden_early(2)
-    forward(wide_cuts + 2)
-    forward_again(wide_cuts)
-
-    @pl.when(outside)
-    def _():
-        arrived(relay_out.at[1], relay_recv.at[1])
-
-    for s in range(3):
-        hidden_late(s)
-    forward(wide_cuts + 3)
-    forward_again(wide_cuts + 1)
-    for n, r in enumerate((g_all, u_all)):
-        arrived(r.at[3, grp], cross_wide.at[0, n])
-        arrived(r.at[3, 1 - grp], cross_wide.at[1, n])
-    hidden_early(3)
-    hidden_late(3)
-
-    def outer_of(c):
-        cols = cols_of(c, fine)
-        return send(
-            outer_out.at[:, :, cols], outer_in.at[:, :, cols], outer_send, outer_recv.at[c], {"ep": side}
-        )
-
-    def final(c):
-        cols = cols_of(c, fine)
-        for way in range(2):
-            cross_of(way, wide_cuts + c).wait_recv()
-        down = jnp.concatenate(
-            [d_all[s, :, :, cols].reshape(units, deep // fine) for s in range(4)], axis=0
-        )
-        whole = jnp.dot(hid[...], down, preferred_element_type=F32).astype(BF16)
-        for slot in range(2):
-            first = (2 + slot) * capacity
-            outer_out[slot, :, cols] = whole[first : first + capacity]
-
-        @pl.when(outside)
-        def _():
-            outer_of(c).start()
-
-        back_out[:, cols] = whole[capacity : 2 * capacity]
-        back_in[0, :, cols] = whole[:capacity]
-
-    def home_of(slot, c):
-        return send(
-            dense_out.at[slot, :, cols_of(c, fine)],
-            dense_back.at[:, cols_of(c, fine)],
-            home_send.at[slot],
-            home_recv.at[c],
-            {"ep": far[slot]},
-        )
-
-    def weigh(at, near_rows, far_rows):
-        gate = gate_cols[at]
-        here = jnp.dot(sel_back[2 * at], near_rows, preferred_element_type=F32)
-        there = jnp.dot(sel_back[2 * at + 1], far_rows, preferred_element_type=F32)
-        return gate[:, 0:1] * here + gate[:, 1:2] * there
-
-    def return_home(c):
-        cols = cols_of(c, fine)
-
-        @pl.when(inner)
-        def _():
-            outer_of(c).wait_recv()
-            for slot in range(2):
-                dense_out[slot, :, cols] = weigh(
-                    1 + slot, outer_out[slot, :, cols], outer_in[slot, :, cols]
-                ).astype(BF16)
-                home_of(slot, c).start()
+        hidden(s, 3, 4)
+
+    def half_of(s, g):
+        cols = pl.ds(pl.multiple_of(g * depth, depth), depth)
+        flat = rows_in[0:3, :, cols].reshape(3 * capacity, depth)
+        gate = jnp.dot(flat, g_all[s, g].reshape(depth, units), preferred_element_type=F32)
+        up = jnp.dot(flat, u_all[s, g].reshape(depth, units), preferred_element_type=F32)
+        return gate, up
+
+    def hidden_first(s):
+        gate, up = half_of(s, grp)
+        sofar[s - 2, 0] = gate
+        sofar[s - 2, 1] = up
+
+    def hidden_second(s):
+        gate, up = half_of(s, 1 - grp)
+        activate(sofar[s - 2, 0] + gate, sofar[s - 2, 1] + up, s, rows_of(0, 3))
 
     block = (span, span)
     key_sub = lax.broadcasted_iota(jnp.int32, block, 0)
@@ -615,11 +546,10 @@
     after = (key_sub > key_lane).astype(BF16)
     past = key_lane < key_sub
 
-    def attend(i):
-        result = []
-        for h in range(heads):
+    def attend(i, heads_now):
+        for h in heads_now:
             cols = slice(h * head, (h + 1) * head)
-            query = qkv_all[i, 0][:, cols]
+            query = qkv_all[i, 0][:, cols] * BF16(head**-0.5)
             for j in range(i, -1, -1):
                 z = lax.dot_general(
                     query,
@@ -627,10 +557,9 @@
                     (((1,), (1,)), ((), ())),
                     preferred_element_type=F32,
                 )
-                z = z * head ** (-0.5) + bias_rows[j, pl.ds(me * heads + h, 1), :]
-                soft = jnp.log1p(jnp.exp(-jnp.abs(z)))
-                rest = -(jnp.maximum(z, 0.0) + soft)
-                stop = jnp.minimum(z, 0.0) - soft
+                z = z + bias_rows[j, pl.ds(me * heads + h, 1), :]
+                stop = jnp.minimum(z, 0.0) - jnp.log(1.0 + jnp.exp(jnp.minimum(z, -z)))
+                rest = stop - z
                 if j == i:
                     rest = jnp.where(past, rest, 0.0)
                 hi = rest.astype(BF16)
@@ -651,13 +580,13 @@
                 if j > 0:
                     tally = jnp.sum(rest, axis=1, keepdims=True)
                     carry = tally if j == i else carry + tally
-            result.append(total)
-        got = jnp.concatenate(result, axis=1).astype(BF16)
-        att_send[i] = got
+            att_send[i, :, cols] = total.astype(BF16)
+        if heads_now[-1] != heads - 1:
+            return
 
         @pl.when(me == i)
         def _():
-            att_all[i] = got
+            att_all[i] = att_send[i]
 
         @pl.when(me != i)
         def _():
@@ -666,44 +595,205 @@
     def att_of(i, j):
         return send(att_send.at[i], att_all.at[j], att_ssem.at[i], att_rsem.at[j], {"ep": i})
 
+    def packs_here():
+        for copy in mine:
+            copy.wait()
+        loads[8].wait()
+        for r in range(1, ep):
+            source = lax.rem(me + r, ep)
+            arrived(qkv_all.at[source], pack_recv.at[source])
+            arrived(bias_all.at[source], bias_recv.at[source])
+        bias_rows[...] = bias_all[...].astype(F32)
+
+    firsts, lasts = tuple(range(heads // 2)), tuple(range(heads // 2, heads))
+    everyone = firsts + lasts
+    W = wide_cuts
+    lag = 3
+    near_at = (4, 7, 10)
+    for n in range(W):
+        if n % 2 == 0 and 2 <= n < 2 + 2 * parts:
+            relay(0, n // 2 - 1)
+        forward(n)
+        if n >= lag:
+            forward_again(n - lag)
+        if n in near_at:
+            nears[near_at.index(n)].start()
+        if n == 9:
+
+            @pl.when(inner)
+            def _():
+                pack(2, side)
+
+        if n == 13:
+            packs_here()
+            attend(3, firsts)
+        if n == 14:
+            attend(3, lasts)
+        if n == 15:
+            relay(1, 0)
+            attend(0, everyone)
+
+    forward_again(W - 3)
+    forward(W)
+    attend(2, everyone)
+    relay(1, 1)
+    forward(W + 1)
+    forward_again(W - 2)
+    side_rows.wait_recv()
+
+    @pl.when(outside)
+    def _():
+        arrived(relay_out.at[0], relay_recv.at[0])
+
+    hidden_early(0)
+    forward(W + 2)
+    for copy in nears:
+        copy.wait_recv()
+    hidden_early(1)
+    forward_again(W - 1)
+    for n, r in enumerate((g_all, u_all)):
+        arrived(r.at[3, grp], cross_wide.at[0, n])
+    hidden_first(2)
+    hidden_first(3)
+    forward(W + 3)
+    hidden_second(2)
+    forward_again(W)
+    relay(1, 2)
+    forward(W + 4)
+    for n, r in enumerate((g_all, u_all)):
+        arrived(r.at[3, 1 - grp], cross_wide.at[1, n])
+    hidden_second(3)
+    forward_again(W + 1)
+
+    def outer_of(slot, c):
+        cols = strip(c)
+        return send(
+            outer_out.at[slot, :, cols],
+            outer_in.at[slot, :, cols],
+            outer_send.at[slot],
+            outer_recv.at[slot, c],
+            {"ep": side},
+        )
+
+    def back_of(cols):
+        return send(
+            back_out.at[:, cols], back_in.at[1, :, cols], back_ssem, back_rsem, {"ep": side}
+        )
+
+    def lower(cols, a, b):
+        down = jnp.concatenate(
+            [d_all[s, :, :, cols].reshape(units, -1) for s in range(4)], axis=0
+        )
+        return jnp.dot(hid[rows_of(a, b)], down, preferred_element_type=F32).astype(BF16)
+
+    def put_far(slot, c, rows):
+        outer_out[slot, :, strip(c)] = rows
+
+        @pl.when(outside)
+        def _():
+            outer_of(slot, c).start()
+
+    def final(c):
+        cols = strip(c)
+        arrived(d_all.at[3, :, :, cols], cross_down.at[c])
+        rows = lower(cols, 0, 3)
+        put_far(0, c, rows[rows_of(2, 3)])
+        back_in[0, :, cols] = rows[rows_of(0, 1)]
+        back_out[:, cols] = rows[rows_of(1, 2)]
+
+        @pl.when(inner)
+        def _():
+            back_of(cols).start()
+
+    def final_late(c):
+        put_far(1, c, lower(strip(c), 3, 4))
+
+    def back_strips(first, last):
+        @pl.when(outside)
+        def _():
+            back_of(slice(strip(first).start, strip(last).stop)).start()
+
+    def home_of(slot, c):
+        return send(
+            dense_out.at[slot, :, strip(c)],
+            dense_back.at[:, strip(c)],
+            home_send.at[slot],
+            home_recv.at[c],
+            {"ep": far[slot]},
+        )
+
+    def weigh(at, near_rows, far_rows):
+        gate = gate_cols[at]
+        here = jnp.dot(sel_back[2 * at], near_rows, preferred_element_type=F32)
+        there = jnp.dot(sel_back[2 * at + 1], far_rows, preferred_element_type=F32)
+        return gate[:, 0:1] * here + gate[:, 1:2] * there
+
+    def return_home(slot, c):
+        cols = strip(c)
+
+        @pl.when(inner)
+        def _():
+            outer_of(slot, c).wait_recv()
+            dense_out[slot, :, cols] = weigh(
+                1 + slot, outer_out[slot, :, cols], outer_in[slot, :, cols]
+            ).astype(BF16)
+            home_of(slot, c).start()
+
     final(0)
-    forward(wide_cuts + 4)
-    forward_again(wide_cuts + 2)
+    forward(W + 5)
+    forward_again(W + 2)
     final(1)
-    forward(wide_cuts + 5)
-    forward_again(wide_cuts + 3)
+    relay(1, 3)
+    attend(1, everyone)
+    forward(W + 6)
+    forward_again(W + 3)
     final(2)
-    forward(wide_cuts + 6)
-    forward_again(wide_cuts + 4)
+    return_home(0, 0)
+    return_home(0, 1)
+    forward(W + 7)
+    forward_again(W + 4)
     final(3)
-    for copy in mine:
-        copy.wait()
-    loads[8].wait()
-    for r in range(1, ep):
-        source = lax.rem(me + r, ep)
-        arrived(qkv_all.at[source], pack_recv.at[source])
-        arrived(bias_all.at[source], bias_recv.at[source])
-    bias_rows[...] = bias_all[...].astype(F32)
-    return_home(0)
-    attend(3)
-    forward(wide_cuts + 7)
-    forward_again(wide_cuts + 5)
+    return_home(0, 2)
+    forward(W + 8)
+    forward_again(W + 5)
     final(4)
-    return_home(1)
-    attend(2)
-    forward_again(wide_cuts + 6)
+    back_strips(0, 1)
+    return_home(0, 3)
+    forward_again(W + 6)
     final(5)
-    return_home(2)
-    attend(1)
-    forward_again(wide_cuts + 7)
+    return_home(0, 4)
+    forward_again(W + 7)
     final(6)
-    return_home(3)
-    attend(0)
+    back_strips(2, 2)
+
+    @pl.when(outside)
+    def _():
+        arrived(relay_out.at[1], relay_recv.at[1])
+
+    hidden_late(0)
+    return_home(0, 5)
+    hidden_late(1)
+    forward_again(W + 8)
     final(7)
-    side_back = send(back_out, back_in.at[1], back_ssem, back_rsem, {"ep": side})
-    side_back.start()
-    for c in range(4, fine):
-        return_home(c)
+    hidden_late(2)
+    return_home(0, 6)
+    hidden_late(3)
+    final(8)
+    back_strips(3, 3)
+    final_late(0)
+    final_late(1)
+    return_home(0, 7)
+    final_late(2)
+    final_late(3)
+    return_home(0, 8)
+    final_late(4)
+    return_home(1, 0)
+    final_late(5)
+    return_home(1, 1)
+    for c in range(6, fine):
+        final_late(c)
+    back_strips(4, fine - 1)
+    return_home(1, 2)
     for j in range(ep):
 
         @pl.when(me != j)
@@ -720,6 +810,8 @@
     ]
     for copy in shares:
         copy.start()
+    for c in range(3, fine):
+        return_home(1, c)
     whole = proj[tp].astype(F32)
     for copy in shares:
         copy.wait_recv()
@@ -748,18 +840,19 @@
 
     for copy in shares:
         copy.wait_send()
-    side_back.wait_recv()
+    arrived(back_out, back_rsem)
     for c in range(fine):
-        cols = cols_of(c, fine)
+        cols = strip(c)
         acc[:, cols] = weigh(0, back_in[0, :, cols], back_in[1, :, cols])
-    side_back.wait_send()
+    drained(back_out, back_ssem)
 
     @pl.when(outside)
     def _():
-        drained(outer_out, outer_send)
+        for slot in range(2):
+            drained(outer_out.at[slot], outer_send.at[slot])
 
     for c in range(fine):
-        cols = cols_of(c, fine)
+        cols = strip(c)
         home_of(0, c).wait_recv()
         out_ref[:, cols] = (acc[:, cols] + dense_back[:, cols].astype(F32)).astype(BF16)
 
@@ -808,7 +901,7 @@
     units = gate_weight.shape[2]
     cuts = 8
     parts = 4
-    fine = 8
+    fine = 9
     lines = 8
     gate = gate_weight.reshape(groups, cuts, deep // (groups * cuts), units)
     up = up_weight.reshape(gate.shape)
@@ -850,6 +943,7 @@
             pltpu.VMEM((2, capacity, deep), BF16),
             pltpu.VMEM((ep, capacity, deep), BF16),
             pltpu.VMEM((ep * capacity, tp * units), BF16),
+            pltpu.VMEM((2, 2, 3 * capacity, units), F32),
             pltpu.VMEM((tokens, deep), F32),
             pltpu.VMEM((capacity, deep), BF16),
             pltpu.VMEM((2, capacity, deep), BF16),
@@ -879,8 +973,8 @@
             dma((ep,)),
             dma(()),
             dma(()),
-            dma(()),
-            dma((fine,)),
+            dma((2,)),
+            dma((2, fine)),
             dma((2,)),
             dma((fine,)),
             dma((tp,)),
@@ -893,7 +987,7 @@
             dma((chunks,)),
             dma((2, 3)),
             dma((2, 2)),
-            dma((2, fine)),
+            dma((fine,)),
         ],
         compiler_params=pltpu.CompilerParams(
             collective_id=0, has_side_effects=True, vmem_limit_bytes=60 * 2**20
@@ -926,7 +1020,9 @@
 def pick_plan(groups, ep, tp, *args):
     heads = args[3].shape[1]
     width = args[0].shape[1] // ep
-    if groups == 2 and tp == 4 and ep == 4 and heads % ep == 0 and width % 128 == 0:
+    head = args[0].shape[1] // heads
+    exact = head & (head - 1) == 0 and head.bit_length() % 2 == 1
+    if groups == 2 and tp == 4 and ep == 4 and heads % ep == 0 and width % 128 == 0 and exact:
         return fused_device(groups, ep, tp, *args)
     return per_device(*args)
 

time: 77.4 us -> 70.6 us (0.912)
  Pallas kernels: 76.6 us -> 69 us
    pallas_call x1, Pallas kernels: 75.7 us -> 68.2 us  [fused_device(): pl.pallas_call(functools.partial(layer_kernel, ep, capacity, cols // head...]
where the time goes in v2:
time: 70.6 us; the launch traced here: 69.8 us
  Pallas kernels  69 us (98%)
  between operations  0.8 us (1%)
    pallas_call x1, Pallas kernels, fused_device(): pl.pallas_call(functools.partial(layer_kernel, ep, capacity, cols // head...  68.2 us

profile of v2, /device:TPU:0, one launch (start us, length us, event | category | flops | bytes accessed | tf_op | source)
XLA Modules:
  0.0 69.8 jit_solution(6131451886798889467)
XLA Ops:
  0.6 68.2 %shard_map.140 = (bf16[32,2048]{1,0:T(8,128)(2,1)S(1)}, bf16[128,2048]{1,0:T(8,128)(2,1)S(1)}) custom-call(bf16[128,512]{1,0:T(8,128)(2,1)} %q_ref.1, bf16[128,512]{1,0:T(8,128)(2,1)} %k_ref.1, bf16[128,512]{1,0:T(8,128)(2,1)} %v_ref.1, bf16[8,128]{1,0:T(8,128)(2,1)} %bitcast.13, bf16[512,2048]{1,0:T(8,128)(2,1)} %ow_ref.1, f32[1,2048]{1,0:T(1,128)} %bitcast.11, ...), custom_call_target="tpu_custom_call" | custom-call | tf_op jit(solution)/shard_map/pallas_call | solution.py:913
  68.8 0.8 %shard_map.141 = (bf16[32,2048]{1,0:T(8,128)(2,1)}, bf16[128,2048]{1,0:T(8,128)(2,1)}) custom-call(bf16[32,2048]{1,0:T(8,128)(2,1)S(1)} %get-tuple-element.4.mixed_ref, bf16[128,2048]{1,0:T(8,128)(2,1)S(1)} %get-tuple-element.5.out_ref), custom_call_target="tpu_custom_call" | custom-call | tf_op jit(solution)/shard_map/pallas_call | solution.py:1011

commit v3 on v2

--- a/solution.py
+++ b/solution.py
@@ -210,6 +210,8 @@
     meta_in,
     normed_ref,
     dense_in,
+    beside,
+    beside_meta,
     sel,
     sel_back,
     gate_cols,
@@ -241,6 +243,10 @@
     meta_recv,
     dense_send,
     dense_recv,
+    pass_send,
+    beside_recv,
+    beside_meta_send,
+    beside_meta_recv,
     relay_send,
     relay_recv,
     att_ssem,
@@ -274,7 +280,7 @@
     tokens, deep = x_ref.shape
     top = ids_ref.shape[0]
     parts = dense_recv.shape[1]
-    fine = home_recv.shape[0]
+    fine = outer_recv.shape[1]
     wide_cuts = 2 * g_ref.shape[1]
 
     half = me // 2
@@ -282,7 +288,8 @@
     inner = is_inner == 1
     outside = is_inner == 0
     side = me + 1 - 2 * (me % 2)
-    far = (3 * (1 - half), 2 - half)
+    my_slot = 1 - is_inner
+    far = (2 - half, 3 * (1 - half))
 
     loads = [
         pltpu.make_async_copy(s, t, load_sem.at[n])
@@ -371,14 +378,14 @@
         return send(
             piece_of(n, 0, grp),
             piece_of(n, 2, grp),
-            x_send.at[kind_of(n)],
+            x_send,
             x_recv.at[n],
             {"tp": mates[2]},
         )
 
     loads[4].wait()
     over_x(0).start()
-    send(meta, meta_in.at[is_inner], meta_send, meta_recv.at[is_inner], {"ep": far[1]}).start()
+    send(meta, meta_in.at[my_slot], meta_send, meta_recv.at[my_slot], {"ep": far[0]}).start()
 
     def dense_of(slot, c):
         return send(
@@ -386,7 +393,7 @@
             dense_in.at[slot, :, cols_of(c)],
             dense_send,
             dense_recv.at[slot, c],
-            {"ep": far[1]},
+            {"ep": far[0]},
         )
 
     pieces = (q_ref, k_ref, v_ref)
@@ -401,21 +408,33 @@
                 pack_recv.at[me],
                 {"ep": dest},
             ).start()
-        send(bias_ref, bias_all.at[me], bias_send.at[r], bias_recv.at[me], {"ep": dest}).start()
+        send(bias_ref, bias_all.at[me], bias_send, bias_recv.at[me], {"ep": dest}).start()
+
+    pack(0, far[0])
+    pack(1, far[1])
+    pack(2, side)
 
     @pl.when(inner)
     def _():
-        pack(0, far[1])
-        pack(1, far[0])
-
-    for c in range(parts):
-        dense_of(is_inner, c).start()
+        for c in range(parts):
+            dense_of(0, c).start()
+
+    def beside_of(c):
+        return send(
+            normed_ref.at[:, cols_of(c)],
+            beside.at[:, cols_of(c)],
+            dense_send,
+            beside_recv.at[c],
+            {"ep": side},
+        )
+
+    beside_table = send(meta, beside_meta, beside_meta_send, beside_meta_recv, {"ep": side})
 
     @pl.when(outside)
     def _():
-        pack(0, far[1])
-        pack(1, far[0])
-        pack(2, side)
+        beside_table.start()
+        for c in range(parts):
+            beside_of(c).start()
 
     loads[5].wait()
     for n in range(1, wide_cuts):
@@ -424,7 +443,7 @@
     for n in range(wide_cuts, chunks):
         over_x(n).start()
     nears = [
-        send(r.at[0], r.at[1], near_send.at[n], near_recv.at[n], mate)
+        send(r.at[0], r.at[1], near_send, near_recv.at[n], mate)
         for n, r in enumerate((g_all, u_all, d_all))
     ]
     square = (tokens, tokens)
@@ -459,13 +478,34 @@
         rows_in[0, :, cols_of(c)] = both[:capacity]
         outbound[:, cols_of(c)] = both[capacity:]
     side_rows = send(outbound, rows_in.at[1], row_send, row_recv, {"ep": side})
-    side_rows.start()
+
+    @pl.when(inner)
+    def _():
+        side_rows.start()
+
+    def take(c):
+        @pl.when(inner)
+        def _():
+            if c == 0:
+                beside_table.wait_recv()
+                route(beside_meta[...], 3)
+            beside_of(c).wait_recv()
+            send(
+                beside.at[:, cols_of(c)],
+                dense_in.at[1, :, cols_of(c)],
+                pass_send,
+                dense_recv.at[1, c],
+                {"ep": far[0]},
+            ).start()
+            rows_in[1, :, cols_of(c)] = jnp.dot(
+                sel[3, :capacity], beside[:, cols_of(c)], preferred_element_type=F32
+            ).astype(BF16)
 
     def relay_of(slot, c):
         return send(
             relay_out.at[slot, :, cols_of(c)],
             rows_in.at[2 + slot, :, cols_of(c)],
-            relay_send.at[slot],
+            relay_send,
             relay_recv.at[slot],
             {"ep": side},
         )
@@ -487,7 +527,7 @@
         send(
             piece_of(n, 2, grp),
             piece_of(n, 2, grp),
-            y_send.at[kind_of(n)],
+            y_send,
             y_recv.at[n],
             {"grp": 1 - grp},
         ).start()
@@ -496,7 +536,7 @@
     def cross_of(way, n):
         g = grp if way == 0 else 1 - grp
         landed = cross_wide.at[way, n % 2] if n < wide_cuts else cross_down.at[n - wide_cuts]
-        return send(piece_of(n, 2, g), piece_of(n, 3, g), cross_send.at[way, kind_of(n)], landed, mate)
+        return send(piece_of(n, 2, g), piece_of(n, 3, g), cross_send, landed, mate)
 
     def forward_again(n):
         arrived(piece_of(n, 2, 1 - grp), y_recv.at[n])
@@ -518,8 +558,11 @@
         up = jnp.dot(flat, u_all[s].reshape(deep, units), preferred_element_type=F32)
         activate(gate, up, s, rows_of(a, b))
 
-    def hidden_early(s):
-        hidden(s, 0, 3)
+    def hidden_near(s):
+        hidden(s, 0, 2)
+
+    def hidden_first_slot(s):
+        hidden(s, 2, 3)
 
     def hidden_late(s):
         hidden(s, 3, 4)
@@ -593,7 +636,7 @@
             att_of(i, me).start()
 
     def att_of(i, j):
-        return send(att_send.at[i], att_all.at[j], att_ssem.at[i], att_rsem.at[j], {"ep": i})
+        return send(att_send.at[i], att_all.at[j], att_ssem, att_rsem.at[j], {"ep": i})
 
     def packs_here():
         for copy in mine:
@@ -609,56 +652,66 @@
     everyone = firsts + lasts
     W = wide_cuts
     lag = 3
-    near_at = (4, 7, 10)
+    near_at = (2, 4, 10)
     for n in range(W):
-        if n % 2 == 0 and 2 <= n < 2 + 2 * parts:
-            relay(0, n // 2 - 1)
         forward(n)
         if n >= lag:
             forward_again(n - lag)
+        if n in (7, 9, 11, 13):
+            relay(0, (n - 7) // 2)
         if n in near_at:
             nears[near_at.index(n)].start()
-        if n == 9:
-
-            @pl.when(inner)
-            def _():
-                pack(2, side)
-
-        if n == 13:
+        if n == 5:
             packs_here()
             attend(3, firsts)
+        if n == 6:
+            attend(3, lasts)
+        if n == 7:
+            attend(0, everyone)
+        if n == 8:
+            attend(2, everyone)
+        if n == 9:
+            attend(1, everyone)
+        if n == 10:
+            take(0)
+            take(1)
+        if n == 12:
+            take(2)
         if n == 14:
-            attend(3, lasts)
+            take(3)
+
+            @pl.when(outside)
+            def _():
+                side_rows.wait_recv()
+
+            hidden_near(0)
         if n == 15:
-            relay(1, 0)
-            attend(0, everyone)
+            for copy in nears:
+                copy.wait_recv()
+            hidden_near(1)
 
     forward_again(W - 3)
     forward(W)
-    attend(2, everyone)
-    relay(1, 1)
     forward(W + 1)
-    forward_again(W - 2)
-    side_rows.wait_recv()
 
     @pl.when(outside)
     def _():
         arrived(relay_out.at[0], relay_recv.at[0])
 
-    hidden_early(0)
+    hidden_first_slot(0)
+    forward_again(W - 2)
+    hidden_first_slot(1)
+    relay(1, 0)
     forward(W + 2)
-    for copy in nears:
-        copy.wait_recv()
-    hidden_early(1)
-    forward_again(W - 1)
     for n, r in enumerate((g_all, u_all)):
         arrived(r.at[3, grp], cross_wide.at[0, n])
     hidden_first(2)
     hidden_first(3)
     forward(W + 3)
+    forward_again(W - 1)
     hidden_second(2)
     forward_again(W)
-    relay(1, 2)
+    relay(1, 1)
     forward(W + 4)
     for n, r in enumerate((g_all, u_all)):
         arrived(r.at[3, 1 - grp], cross_wide.at[1, n])
@@ -670,14 +723,22 @@
         return send(
             outer_out.at[slot, :, cols],
             outer_in.at[slot, :, cols],
-            outer_send.at[slot],
+            outer_send,
             outer_recv.at[slot, c],
             {"ep": side},
         )
 
+    thirds = [
+        slice(strip(a).start, strip(b).stop) for a, b in ((0, 3), (4, fine - 3), (fine - 2, fine - 1))
+    ]
+
     def back_of(cols):
         return send(
-            back_out.at[:, cols], back_in.at[1, :, cols], back_ssem, back_rsem, {"ep": side}
+            back_out.at[:, cols],
+            back_in.at[1, :, cols],
+            back_ssem,
+            back_rsem.at[sum(cols.start >= e.start for e in thirds[1:])],
+            {"ep": side},
         )
 
     def lower(cols, a, b):
@@ -692,6 +753,8 @@
         @pl.when(outside)
         def _():
             outer_of(slot, c).start()
+
+    held = 3
 
     def final(c):
         cols = strip(c)
@@ -701,9 +764,11 @@
         back_in[0, :, cols] = rows[rows_of(0, 1)]
         back_out[:, cols] = rows[rows_of(1, 2)]
 
-        @pl.when(inner)
-        def _():
-            back_of(cols).start()
+        if c > held:
+
+            @pl.when(inner)
+            def _():
+                back_of(cols).start()
 
     def final_late(c):
         put_far(1, c, lower(strip(c), 3, 4))
@@ -717,8 +782,8 @@
         return send(
             dense_out.at[slot, :, strip(c)],
             dense_back.at[:, strip(c)],
-            home_send.at[slot],
-            home_recv.at[c],
+            home_send,
+            home_recv.at[c // (fine - 1)],
             {"ep": far[slot]},
         )
 
@@ -743,17 +808,22 @@
     forward(W + 5)
     forward_again(W + 2)
     final(1)
-    relay(1, 3)
-    attend(1, everyone)
     forward(W + 6)
     forward_again(W + 3)
+    relay(1, 2)
     final(2)
     return_home(0, 0)
+    relay(1, 3)
     return_home(0, 1)
     forward(W + 7)
     forward_again(W + 4)
     final(3)
     return_home(0, 2)
+
+    @pl.when(inner)
+    def _():
+        back_of(slice(0, strip(held).stop)).start()
+
     forward(W + 8)
     forward_again(W + 5)
     final(4)
@@ -764,35 +834,33 @@
     return_home(0, 4)
     forward_again(W + 7)
     final(6)
-    back_strips(2, 2)
+    return_home(0, 5)
 
     @pl.when(outside)
     def _():
         arrived(relay_out.at[1], relay_recv.at[1])
 
     hidden_late(0)
-    return_home(0, 5)
     hidden_late(1)
     forward_again(W + 8)
     final(7)
+    return_home(0, 6)
     hidden_late(2)
-    return_home(0, 6)
     hidden_late(3)
     final(8)
-    back_strips(3, 3)
+    return_home(0, 7)
+    return_home(0, 8)
     final_late(0)
     final_late(1)
-    return_home(0, 7)
     final_late(2)
     final_late(3)
-    return_home(0, 8)
-    final_late(4)
     return_home(1, 0)
-    final_late(5)
     return_home(1, 1)
-    for c in range(6, fine):
+    for c in range(4, fine):
         final_late(c)
-    back_strips(4, fine - 1)
+    back_strips(2, 3)
+    back_strips(4, fine - 3)
+    back_strips(fine - 2, fine - 1)
     return_home(1, 2)
     for j in range(ep):
 
@@ -821,46 +889,44 @@
     scale = lax.rsqrt(jnp.mean(whole * whole, axis=-1, keepdims=True) + 1e-06)
     mixed_ref[...] = (whole * scale * mix_own[...]).astype(BF16)
     drained(normed_ref, dense_send)
-    for n, r in enumerate((g_all, u_all, d_all)):
-        drained(r.at[0, grp], x_send.at[n])
-        drained(r.at[2, grp], y_send.at[n])
-        drained(r.at[2, grp], cross_send.at[0, n])
-        drained(r.at[2, 1 - grp], cross_send.at[1, n])
-        nears[n].wait_send()
+    drained(g_all.at[pl.ds(0, 3), 0], x_send)
+    drained(g_all.at[pl.ds(0, 3), 0], y_send)
+    drained(g_all.at[pl.ds(0, 3)], cross_send)
+    drained(g_all.at[pl.ds(0, 3)], near_send)
     drained(qkv_all.at[pl.ds(0, 3)], pack_send)
-    for r in range(ep - 1):
-        drained(bias_all.at[0], bias_send.at[r])
-    side_rows.wait_send()
+    drained(bias_all.at[pl.ds(0, ep - 1)], bias_send)
+
+    @pl.when(inner)
+    def _():
+        side_rows.wait_send()
+        drained(beside, pass_send)
+
+    @pl.when(outside)
+    def _():
+        beside_table.wait_send()
+
     drained(meta, meta_send)
-    for i in range(ep):
-
-        @pl.when(me != i)
-        def _():
-            drained(att_send.at[i], att_ssem.at[i])
+    drained(att_send.at[pl.ds(0, ep - 1)], att_ssem)
 
     for copy in shares:
         copy.wait_send()
-    arrived(back_out, back_rsem)
-    for c in range(fine):
-        cols = strip(c)
+    for n, cols in enumerate(thirds):
+        arrived(back_in.at[1, :, cols], back_rsem.at[n])
         acc[:, cols] = weigh(0, back_in[0, :, cols], back_in[1, :, cols])
     drained(back_out, back_ssem)
 
     @pl.when(outside)
     def _():
-        for slot in range(2):
-            drained(outer_out.at[slot], outer_send.at[slot])
-
-    for c in range(fine):
-        cols = strip(c)
-        home_of(0, c).wait_recv()
+        drained(outer_out, outer_send)
+
+    for n, cols in enumerate((slice(0, strip(fine - 1).start), strip(fine - 1))):
+        arrived(dense_back.at[:, cols], home_recv.at[n])
         out_ref[:, cols] = (acc[:, cols] + dense_back[:, cols].astype(F32)).astype(BF16)
 
     @pl.when(inner)
     def _():
-        for slot in range(2):
-            drained(relay_out.at[slot], relay_send.at[slot])
-            drained(dense_out.at[slot], home_send.at[slot])
+        drained(relay_out, relay_send)
+        drained(dense_out, home_send)
 
 
 def settle_kernel(mixed_ref, out_ref, mixed_to, out_to, sems):
@@ -936,9 +1002,11 @@
             pltpu.VMEM((2, lines, tokens), F32),
             pltpu.VMEM((tokens, deep), BF16),
             pltpu.VMEM((2, tokens, deep), BF16),
-            pltpu.VMEM((3, 2 * capacity, tokens), BF16),
-            pltpu.VMEM((6, tokens, capacity), BF16),
-            pltpu.VMEM((3, tokens, tokens), F32),
+            pltpu.VMEM((tokens, deep), BF16),
+            pltpu.VMEM((lines, tokens), F32),
+            pltpu.VMEM((4, 2 * capacity, tokens), BF16),
+            pltpu.VMEM((8, tokens, capacity), BF16),
+            pltpu.VMEM((4, tokens, tokens), F32),
             pltpu.VMEM((capacity, deep), BF16),
             pltpu.VMEM((2, capacity, deep), BF16),
             pltpu.VMEM((ep, capacity, deep), BF16),
@@ -959,33 +1027,37 @@
             dma(()),
             dma(()),
             dma((ep,)),
+            dma(()),
             dma((ep,)),
+            dma(()),
+            dma(()),
+            dma(()),
+            dma((2,)),
+            dma(()),
+            dma((2, parts)),
+            dma(()),
+            dma((parts,)),
+            dma(()),
+            dma(()),
+            dma(()),
+            dma((2,)),
+            dma(()),
             dma((ep,)),
             dma(()),
-            dma(()),
+            dma((3,)),
+            dma(()),
+            dma((2, fine)),
             dma(()),
             dma((2,)),
-            dma(()),
-            dma((2, parts)),
-            dma((2,)),
-            dma((2,)),
-            dma((ep,)),
-            dma((ep,)),
-            dma(()),
-            dma(()),
-            dma((2,)),
-            dma((2, fine)),
-            dma((2,)),
-            dma((fine,)),
             dma((tp,)),
             dma((tp,)),
+            dma(()),
             dma((3,)),
-            dma((3,)),
-            dma((3,)),
+            dma(()),
             dma((chunks,)),
-            dma((3,)),
+            dma(()),
             dma((chunks,)),
-            dma((2, 3)),
+            dma(()),
             dma((2, 2)),
             dma((fine,)),
         ],

time: 70.6 us -> 69.2 us (0.980)
    pallas_call x1, Pallas kernels: 68.2 us -> 67.4 us  [fused_device(): pl.pallas_call(functools.partial(layer_kernel, ep, capacity, cols // head...]
where the time goes in v3:
time: 69.2 us; the launch traced here: 69.1 us
  Pallas kernels  68.3 us (99%)
  between operations  0.8 us (1%)
    pallas_call x1, Pallas kernels, fused_device(): pl.pallas_call(functools.partial(layer_kernel, ep, capacity, cols // head...  67.4 us

profile of v3, /device:TPU:0, one launch (start us, length us, event | category | flops | bytes accessed | tf_op | source)
XLA Modules:
  0.0 69.1 jit_solution(12538651735085775966)
XLA Ops:
  0.6 67.4 %shard_map.140 = (bf16[32,2048]{1,0:T(8,128)(2,1)S(1)}, bf16[128,2048]{1,0:T(8,128)(2,1)S(1)}) custom-call(bf16[128,512]{1,0:T(8,128)(2,1)} %q_ref.1, bf16[128,512]{1,0:T(8,128)(2,1)} %k_ref.1, bf16[128,512]{1,0:T(8,128)(2,1)} %v_ref.1, bf16[8,128]{1,0:T(8,128)(2,1)} %bitcast.13, bf16[512,2048]{1,0:T(8,128)(2,1)} %ow_ref.1, f32[1,2048]{1,0:T(1,128)} %bitcast.11, ...), custom_call_target="tpu_custom_call" | custom-call | tf_op jit(solution)/shard_map/pallas_call | solution.py:979
  68.1 0.8 %shard_map.141 = (bf16[32,2048]{1,0:T(8,128)(2,1)}, bf16[128,2048]{1,0:T(8,128)(2,1)}) custom-call(bf16[32,2048]{1,0:T(8,128)(2,1)S(1)} %get-tuple-element.4.mixed_ref, bf16[128,2048]{1,0:T(8,128)(2,1)S(1)} %get-tuple-element.5.out_ref), custom_call_target="tpu_custom_call" | custom-call | tf_op jit(solution)/shard_map/pallas_call | solution.py:1083

commit v4 on v3

--- a/solution.py
+++ b/solution.py
@@ -712,7 +712,6 @@
     hidden_second(2)
     forward_again(W)
     relay(1, 1)
-    forward(W + 4)
     for n, r in enumerate((g_all, u_all)):
         arrived(r.at[3, 1 - grp], cross_wide.at[1, n])
     hidden_second(3)
@@ -805,9 +804,10 @@
             home_of(slot, c).start()
 
     final(0)
+    forward(W + 4)
+    final(1)
     forward(W + 5)
     forward_again(W + 2)
-    final(1)
     forward(W + 6)
     forward_again(W + 3)
     relay(1, 2)

time: 69.2 us -> 69.9 us (1.010)
  no operation moved by 1% of the time
where the time goes in v4:
time: 69.9 us; the launch traced here: 69.7 us
  Pallas kernels  68.9 us (99%)
  between operations  0.8 us (1%)
    pallas_call x1, Pallas kernels, fused_device(): pl.pallas_call(functools.partial(layer_kernel, ep, capacity, cols // head...  68.1 us

profile of v4, /device:TPU:0, one launch (start us, length us, event | category | flops | bytes accessed | tf_op | source)
XLA Modules:
  0.0 69.7 jit_solution(14717039131806369807)
XLA Ops:
  0.6 68.1 %shard_map.140 = (bf16[32,2048]{1,0:T(8,128)(2,1)S(1)}, bf16[128,2048]{1,0:T(8,128)(2,1)S(1)}) custom-call(bf16[128,512]{1,0:T(8,128)(2,1)} %q_ref.1, bf16[128,512]{1,0:T(8,128)(2,1)} %k_ref.1, bf16[128,512]{1,0:T(8,128)(2,1)} %v_ref.1, bf16[8,128]{1,0:T(8,128)(2,1)} %bitcast.13, bf16[512,2048]{1,0:T(8,128)(2,1)} %ow_ref.1, f32[1,2048]{1,0:T(1,128)} %bitcast.11, ...), custom_call_target="tpu_custom_call" | custom-call | tf_op jit(solution)/shard_map/pallas_call | solution.py:979
  68.7 0.8 %shard_map.141 = (bf16[32,2048]{1,0:T(8,128)(2,1)}, bf16[128,2048]{1,0:T(8,128)(2,1)}) custom-call(bf16[32,2048]{1,0:T(8,128)(2,1)S(1)} %get-tuple-element.4.mixed_ref, bf16[128,2048]{1,0:T(8,128)(2,1)S(1)} %get-tuple-element.5.out_ref), custom_call_target="tpu_custom_call" | custom-call | tf_op jit(solution)/shard_map/pallas_call | solution.py:1083
